TPU v7x, 512 devices: a whole 4x8x8 slice. The times are simulated.
512 devices in a mesh: sp: 128 (over z, y, core), tp: 4 (over x).
Axes of the slice: x: 4, y: 8, z: 8, core: 2. Of those that a mesh axis runs over, the one named last changes fastest.
Arguments:
- tokens_in: bfloat16 [32768, 2048], P('sp'), may hold values from -6 to 6
- norm_gain: float32 [2048], replicated, may hold values from 0.1 to 1.9
- rec_query_weight: bfloat16 [2048, 1024], P('sp', 'tp'), may hold values from -0.125 to 0.125
- rec_forget_weight: bfloat16 [2048, 1024], P('sp', 'tp'), may hold values from -0.125 to 0.125
- rec_input_weight: bfloat16 [2048, 1024], P('sp', 'tp'), may hold values from -0.125 to 0.125
- att_query_weight: bfloat16 [2048, 1024], P('sp', 'tp'), may hold values from -0.18991481 to 0.18991481
- att_key_weight: bfloat16 [2048, 1024], P('sp', 'tp'), may hold values from -0.18991481 to 0.18991481
- att_value_weight: bfloat16 [2048, 1024], P('sp', 'tp'), may hold values from -0.125 to 0.125
- recurrence_output_weight: bfloat16 [1024, 2048], P('tp'), may hold values from -0.125 to 0.125
- out_att_weight: bfloat16 [1024, 2048], P('tp'), may hold values from -0.125 to 0.125
- floor_gap: float32 [1024], P('tp'), may hold values from 0 to 0.1
- decay_shift: float32 [8, 32768], P('tp', 'sp'), may hold values from -1.5 to 0
- rec_gain: float32 [128], replicated, may hold values from 0.1 to 1.9
- att_gain: float32 [128], replicated, may hold values from 0.1 to 1.9
- lambda_head: float32 [8], P('tp'), may hold values from 0.3 to 0.8
Outputs:
- mixed: bfloat16 [32768, 2048], P('sp')
All inputs are finite; a program needn't handle non-finite values.
Results may differ from a plain program's by a relative error of at most 0.015.
Values may be sent and summed in bfloat16 or wider, within the bound.
A program may use at most 128 MiB of HBM per device.

v0:
```python
import jax
import jax.numpy as jnp
from jax import lax
from jax.sharding import Mesh
from jax.sharding import PartitionSpec as P

REC_KEY = 128
REC_VAL = 128
PAIR = 64
ATT_VAL = 128
BLOCK = 64
SP = ("sp_0", "sp_1", "sp_2")


RECUR_EPSILON = 1e-06
ATTEND_EPSILON = 1e-05
ROTARY_BASE = 10000.0


def sent_together(arrays, axis, dim, along):
    widths = [a.shape[along] for a in arrays]
    both = jnp.concatenate(arrays, axis=along)
    result = lax.all_gather(both, axis, axis=dim, tiled=True)
    return tuple(jnp.split(result, [sum(widths[:k]) for k in range(1, len(widths))], axis=along))


def filled_with(array, identity):
    return jax.tree.map(
        lambda part, zero: jnp.zeros_like(part) + jnp.asarray(zero, part.dtype), array, identity
    )


def entering(array, axes, combine, identity):
    before = start = filled_with(array, identity)
    total = array
    for axis in reversed(axes):
        count, position = (lax.axis_size(axis), lax.axis_index(axis))
        pieces = jax.tree.map(
            lambda part, kind: lax.all_gather(part.astype(kind), axis),
            total,
            (jnp.bfloat16, jnp.bfloat16),
        )
        inside, total = (start, start)
        for k in range(count):
            passed = k < position
            total = combine(
                total, jax.tree.map(lambda part, own: part[k].astype(own.dtype), pieces, array)
            )
            inside = jax.tree.map(lambda new, old: jnp.where(passed, new, old), total, inside)
        before = combine(inside, before)
    return before


def from_behind(block, axis, distance):
    devices = range(lax.axis_size(axis))
    route = [(i - distance, i) for i in devices if i - distance in devices]
    return lax.ppermute(block, axis, route)


def copy_for_each(array, axis):
    count = lax.axis_size(axis)
    return lax.all_to_all(
        jnp.broadcast_to(array[None], (count, *array.shape)), axis, 0, 0, tiled=True
    )


def taken_together(array, axis):
    return copy_for_each(array, axis).astype(jnp.float32).sum(axis=0)


def rms_scale(values, scales, epsilon):
    mean_sq = jnp.mean(values * values, axis=-1, keepdims=True)
    return values * lax.rsqrt(mean_sq + epsilon) * scales


def rotary(values, positions):
    half_width = values.shape[-1] // 2
    frequency = 1.0 / ROTARY_BASE ** (jnp.arange(half_width, dtype=jnp.float32) / half_width)
    angles = positions[:, None] * frequency[None, :]
    cosine = jnp.cos(angles)[:, None, :]
    sine_part = jnp.sin(angles)[:, None, :]
    first_half = values[..., :half_width]
    second_half = values[..., half_width:]
    return jnp.concatenate(
        [
            first_half * cosine - second_half * sine_part,
            second_half * cosine + first_half * sine_part,
        ],
        axis=-1,
    )


def recur_blocks(queries, gate_key_rows, inputs, log_decay, carry_in):
    head_count = queries.shape[0]
    length = queries.shape[1]
    block_count = length // BLOCK

    def split_blocks(array):
        return array.reshape(head_count, block_count, BLOCK, array.shape[-1]).transpose(1, 0, 2, 3)

    causal = jnp.tril(jnp.ones((BLOCK, BLOCK), dtype=bool))

    def advance(carried, bundle):
        q_block, k_block, v_block, g_block = bundle
        cum_log = jnp.cumsum(g_block, axis=1)
        q_decayed = q_block * jnp.exp(cum_log)
        k_growth = k_block * jnp.exp(-cum_log)
        from_past = jnp.einsum("hcd,hde->hce", q_decayed, carried)
        scores = jnp.einsum("htd,hsd->hts", q_decayed, k_growth)
        scores = jnp.where(causal[None], scores, 0.0)
        within = jnp.einsum("hts,hse->hte", scores, v_block)
        end_log = cum_log[:, -1:, :]
        k_to_end = k_block * jnp.exp(end_log - cum_log)
        fresh = jnp.exp(end_log[:, 0, :])[:, :, None] * carried + jnp.einsum(
            "hsd,hse->hde", k_to_end, v_block
        )
        return (fresh, from_past + within)

    final_state, outputs = lax.scan(
        advance,
        carry_in,
        (
            split_blocks(queries),
            split_blocks(gate_key_rows),
            split_blocks(inputs),
            split_blocks(log_decay),
        ),
    )
    return (
        outputs.transpose(1, 0, 2, 3).reshape(head_count, length, inputs.shape[-1]),
        final_state,
    )


def chain(earlier, latter):
    return (earlier[0] * latter[0], latter[0][:, :, None] * earlier[1] + latter[1])


def absorb(running_total, queries, key_rows, value_rows, allowed):
    best_score, sums_exp, weighted = running_total
    scores = jnp.einsum(
        "qhcd,khcd->hcqk", queries, key_rows, preferred_element_type=jnp.float32
    ) * queries.shape[-1] ** (-0.5)
    scores = jnp.where(allowed, scores, -jnp.inf)
    new_best = jnp.maximum(best_score, jnp.max(scores, axis=-1))
    rescale = jnp.exp(best_score - new_best)
    expo_vals = jnp.exp(scores - new_best[..., None])
    sums_exp = sums_exp * rescale + jnp.sum(expo_vals, axis=-1)
    weighted = weighted * rescale[..., None] + jnp.einsum(
        "hcqk,khe->hcqe",
        expo_vals.astype(jnp.bfloat16),
        value_rows,
        preferred_element_type=jnp.float32,
    )
    return (new_best, sums_exp, weighted)


def per_device(
    tokens_in,
    norm_gain,
    rec_query_weight,
    rec_forget_weight,
    rec_input_weight,
    att_query_weight,
    att_key_weight,
    att_value_weight,
    recurrence_output_weight,
    out_att_weight,
    floor_gap,
    decay_shift,
    rec_gain,
    att_gain,
    lambda_head,
):
    tok_rows = tokens_in.shape[0]
    seq_span = lax.axis_size(SP) // 4
    half_span = seq_span // 2
    dev_index = lax.axis_index(SP)
    first_dev = jnp.maximum(0, (dev_index + half_span) // seq_span * seq_span - half_span)
    carry_on = jnp.where(dev_index == first_dev, 0.0, 1.0).astype(jnp.float32)
    gathered = sent_together(
        (
            rec_query_weight,
            rec_forget_weight,
            rec_input_weight,
            att_query_weight,
            att_key_weight,
            att_value_weight,
        ),
        SP,
        0,
        1,
    )
    w_query, w_forget, w_input, w_att_query, w_att_key, w_att_value = gathered
    normed = rms_scale(tokens_in.astype(jnp.float32), norm_gain, RECUR_EPSILON).astype(jnp.bfloat16)

    def project(weight):
        return jnp.dot(normed, weight, preferred_element_type=jnp.float32)

    rec_query = project(w_query).astype(jnp.bfloat16)
    rec_forget = project(w_forget).astype(jnp.bfloat16)
    rec_input = project(w_input).astype(jnp.bfloat16)
    att_heads = w_att_query.shape[1] // (2 * PAIR)
    positions = ((dev_index - first_dev) * tok_rows + jnp.arange(tok_rows, dtype=jnp.int32)).astype(
        jnp.float32
    )
    att_query = (
        rotary(project(w_att_query).reshape(tok_rows, att_heads * 2, PAIR), positions)
        .astype(jnp.bfloat16)
        .reshape(tok_rows, att_heads, 2, PAIR)
    )
    att_key = (
        rotary(project(w_att_key).reshape(tok_rows, att_heads * 2, PAIR), positions)
        .astype(jnp.bfloat16)
        .reshape(tok_rows, att_heads * 2 * PAIR)
    )
    att_value = project(w_att_value).astype(jnp.bfloat16)
    rec_heads = w_query.shape[1] // REC_KEY
    gate_key = floor_gap[None, :] * jax.nn.sigmoid(-rec_forget.astype(jnp.float32))
    log_decay = (
        jnp.log1p(-gate_key).reshape(tok_rows, rec_heads, REC_KEY) + decay_shift.T[:, :, None]
    )

    def by_head(array, column_count):
        return array.reshape(tok_rows, rec_heads, column_count).transpose(1, 0, 2)

    query_heads = by_head(rec_query.astype(jnp.float32), REC_KEY)
    k_heads = by_head(gate_key, REC_KEY)
    v_heads = by_head(rec_input.astype(jnp.float32), REC_VAL)
    g_heads = log_decay.transpose(1, 0, 2)
    zero_state = jnp.zeros((rec_heads, REC_KEY, REC_VAL), jnp.float32)
    local_out, local_state = recur_blocks(query_heads, k_heads, v_heads, g_heads, zero_state)
    reach_logarithm = jnp.cumsum(g_heads, axis=1)
    span_decay = jnp.exp(reach_logarithm[:, -1, :]) * carry_on
    prefix = entering((span_decay, local_state), SP, chain, (jnp.ones_like(span_decay), zero_state))
    incoming_state = prefix[1] * carry_on
    rec_raw = local_out + jnp.einsum(
        "ezp,ept->ezt", query_heads * jnp.exp(reach_logarithm), incoming_state
    )
    rec_mix = (
        rms_scale(rec_raw.transpose(1, 0, 2), rec_gain, RECUR_EPSILON)
        .astype(jnp.bfloat16)
        .reshape(tok_rows, rec_heads * REC_VAL)
    )
    mask_own = jnp.arange(tok_rows)[:, None] >= jnp.arange(tok_rows)[None, :]
    start_state = (
        jnp.full((att_heads, 2, tok_rows), -jnp.inf, jnp.float32),
        jnp.zeros((att_heads, 2, tok_rows), jnp.float32),
        jnp.zeros((att_heads, 2, tok_rows, ATT_VAL), jnp.float32),
    )
    online = absorb(
        start_state,
        att_query,
        att_key.reshape(tok_rows, att_heads, 2, PAIR),
        att_value.reshape(tok_rows, att_heads, ATT_VAL),
        mask_own,
    )
    everything = jnp.array(True)

    def take_block(state_now, keys_flat, values_flat, source):
        key_rows = keys_flat.reshape(tok_rows, att_heads, 2, PAIR)
        value_rows = values_flat.reshape(tok_rows, att_heads, ATT_VAL)
        return lax.cond(
            source >= first_dev,
            lambda held: absorb(held, att_query, key_rows, value_rows, everything),
            lambda held: held,
            state_now,
        )

    buffer_keys, buffer_values = (att_key, att_value)
    for depth_step in range((seq_span - 1).bit_length()):
        stride = 1 << depth_step
        far_keys, far_values = from_behind((buffer_keys, buffer_values), SP, stride)

        def absorb_piece(state_now, bundle):
            counter, piece_keys, piece_values = bundle
            return (
                take_block(
                    state_now, piece_keys, piece_values, dev_index - 2 * stride + 1 + counter
                ),
                None,
            )

        online, unused = lax.scan(
            absorb_piece,
            online,
            (
                jnp.arange(stride, dtype=jnp.int32),
                far_keys.reshape(stride, tok_rows, -1),
                far_values.reshape(stride, tok_rows, -1),
            ),
        )
        if 2 * stride < seq_span:
            buffer_keys = jnp.concatenate([far_keys, buffer_keys], axis=0)
            buffer_values = jnp.concatenate([far_values, buffer_values], axis=0)
    best_score, sums_exp, weighted = online
    att_raw = (
        weighted[:, 0] / sums_exp[:, 0, :, None]
        - lambda_head[:, None, None] * weighted[:, 1] / sums_exp[:, 1, :, None]
    )
    att_mix = (
        rms_scale(att_raw.transpose(1, 0, 2), att_gain, ATTEND_EPSILON)
        .astype(jnp.bfloat16)
        .reshape(tok_rows, att_heads * ATT_VAL)
    )
    partial_value = jnp.dot(rec_mix, recurrence_output_weight, preferred_element_type=jnp.float32)
    partial_value = partial_value + jnp.dot(
        att_mix, out_att_weight, preferred_element_type=jnp.float32
    )
    return (
        taken_together(partial_value.astype(jnp.bfloat16), "tp")
        .astype(jnp.float32)
        .astype(jnp.bfloat16)
    )


def solution(mesh):
    split = Mesh(mesh.devices.reshape(8, 8, 2, mesh.shape["tp"]), ("sp_0", "sp_1", "sp_2", "tp"))
    placed = (
        P(SP, None),
        P(),
        P(SP, "tp"),
        P(SP, "tp"),
        P(SP, "tp"),
        P(SP, "tp"),
        P(SP, "tp"),
        P(SP, "tp"),
        P("tp", None),
        P("tp", None),
        P("tp"),
        P("tp", SP),
        P(),
        P(),
        P("tp"),
    )
    return jax.shard_map(
        per_device, mesh=split, in_specs=placed, out_specs=P(SP, None), check_vma=False
    )
```

profile of v0, /device:TPU:184, one launch (start us, length us, event | category | flops | bytes accessed | tf_op | source)
XLA Modules:
  0.0 635.6 jit_solution(743884662013095067)
XLA Ops:
  14.0 84.1 %all-gather.4.cloned.1.call-done = bf16[2048,1536]{1,0:T(8,128)(2,1)} async-done(((bf16[16,1536]{1,0:T(8,128)(2,1)}), bf16[2048,1536]{1,0:T(8,128)(2,1)}) %all-gather.4.cloned.1.call-update) | async-done | bytes 6291472 | tf_op jit(solution)/shard_map/all_gather | solution.py:23
  98.1 2.2 convolution_convert_fusion.1
  100.4 1.9 convolution_convert_fusion.2
  102.5 1.9 convolution_convert_fusion
  104.4 2.1 collective-permute-start.1
  106.5 2.0 negate_log-plus-one_fusion
  109.5 1.9 fusion.66
  111.4 1.9 fusion.68
  113.5 4.2 collective-permute-start
  118.3 1.8 all-gather
  120.7 13.0 %all_gather.31 = bf16[8,2,128]{2,1,0:T(2,128)(2,1)S(1)} all-gather(bf16[1,2,128]{2,1,0:T(2,128)(2,1)S(1)} %fusion.220), channel_id=1, replica_groups=mesh['sp_0'=8,'sp_1'=8,'sp_2'=2,'tp'=4] {'sp_1'}, dimensions={0}, use_global_device_ids=true | all-gather | bytes 4608 | tf_op jit(solution)/shard_map/all_gather | solution.py:39
  134.3 5.7 while.87
  141.0 6.4 %collective-permute-start.2 = (bf16[512,256]{0,1:T(8,128)(2,1)S(1)}, bf16[512,256]{0,1:T(8,128)(2,1)S(1)}, u32[]{:S(2)}, u32[]{:S(2)}) collective-permute-start(bf16[512,256]{0,1:T(8,128)(2,1)S(1)} %pad_maximum_fusion.4), channel_id=1, source_target_pairs={{0,8},{4,12},{8,16},{12,20},{16,24},{20,28},{24,32},{28,36},{32,40... | collective-permute-start | bytes 786440 | tf_op jit(solution)/shard_map/ppermute | solution.py:57
  148.1 3.6 collective-permute-done.2
  151.8 3.5 collective-permute-start.4
  155.3 5.0 collective-permute-start.3
  160.5 21.0 %collective-permute-done.3 = bf16[512,256]{0,1:T(8,128)(2,1)S(1)} collective-permute-done((bf16[512,256]{0,1:T(8,128)(2,1)S(1)}, bf16[512,256]{0,1:T(8,128)(2,1)S(1)}, u32[]{:S(2)}, u32[]{:S(2)}) %collective-permute-start.3) | collective-permute-done | bytes 262176 | tf_op jit(solution)/shard_map/ppermute | solution.py:57
  181.5 4.2 collective-permute-start.5
  186.8 4.3 collective-permute-start.6
  191.1 12.8 %all_gather.32 = bf16[8,2,128]{2,1,0:T(2,128)(2,1)S(1)} all-gather(bf16[1,2,128]{2,1,0:T(2,128)(2,1)S(1)} %fusion.216), channel_id=1, replica_groups=mesh['sp_0'=8,'sp_1'=8,'sp_2'=2,'tp'=4] {'sp_0'}, dimensions={0}, use_global_device_ids=true | all-gather | bytes 4608 | tf_op jit(solution)/shard_map/all_gather | solution.py:39
  204.3 82.7 %collective-permute-done.5 = bf16[1024,256]{0,1:T(8,128)(2,1)S(1)} collective-permute-done((bf16[1024,256]{0,1:T(8,128)(2,1)S(1)}, bf16[1024,256]{0,1:T(8,128)(2,1)S(1)}, u32[]{:S(2)}, u32[]{:S(2)}) %collective-permute-start.5) | collective-permute-done | bytes 524320 | tf_op jit(solution)/shard_map/ppermute | solution.py:57
  288.1 1.9 collective-permute-start.7
  290.6 1.8 copy.183
  292.4 2.4 constant_dynamic-update-slice_fusion.10
  297.8 44.7 %collective-permute-done.7 = bf16[2048,256]{0,1:T(8,128)(2,1)} collective-permute-done((bf16[2048,256]{0,1:T(8,128)(2,1)}, bf16[2048,256]{0,1:T(8,128)(2,1)}, u32[]{:S(2)}, u32[]{:S(2)}) %collective-permute-start.7) | collective-permute-done | bytes 1048608 | tf_op jit(solution)/shard_map/ppermute | solution.py:57
  342.5 2.3 constant_dynamic-update-slice_fusion.15
  347.9 1.9 collective-permute-start.9
  349.8 1.9 collective-permute-start.8
  351.7 1.9 all-gather.1
  353.8 35.5 %all_gather.35 = bf16[8,2,128,128]{3,2,1,0:T(8,128)(2,1)S(1)} all-gather(bf16[1,2,128,128]{3,2,1,0:T(8,128)(2,1)S(1)} %fusion.124), channel_id=1, replica_groups=mesh['sp_0'=8,'sp_1'=8,'sp_2'=2,'tp'=4] {'sp_1'}, dimensions={0}, use_global_device_ids=true | all-gather | bytes 589824 | tf_op jit(solution)/shard_map/all_gather | solution.py:39
  389.7 71.5 %all_gather.36 = bf16[8,2,128,128]{3,2,1,0:T(8,128)(2,1)S(1)} all-gather(bf16[1,2,128,128]{3,2,1,0:T(8,128)(2,1)S(1)} %fusion.156), channel_id=1, replica_groups=mesh['sp_0'=8,'sp_1'=8,'sp_2'=2,'tp'=4] {'sp_0'}, dimensions={0}, use_global_device_ids=true | all-gather | bytes 589824 | tf_op jit(solution)/shard_map/all_gather | solution.py:39
  466.1 4.8 while.83
  471.4 9.6 %while.84 = (s32[]{:T(128)}, f32[2,2,256]{2,1,0:T(2,128)S(1)}, f32[2,2,256]{2,1,0:T(2,128)S(1)}, f32[2,2,256,128]{3,2,1,0:T(8,128)S(1)}, s32[4]{0:T(128)S(1)}, /...) while((s32[]{:T(128)}, f32[2,2,256]{2,1,0:T(2,128)S(1)}, ...), condition=%wide.region_24.25_spmd, body=%wide.region_19.24_spmd.sunk | while | flops 102500352 | bytes 5177615 | solution.py:284
  485.1 25.3 %while.85 = (s32[]{:T(128)}, f32[2,2,256]{2,1,0:T(2,128)S(1)}, f32[2,2,256]{2,1,0:T(2,128)S(1)}, f32[2,2,256,128]{3,2,1,0:T(8,128)S(1)}, s32[8]{0:T(128)S(1)}, /...) while((s32[]{:T(128)}, f32[2,2,256]{2,1,0:T(2,128)S(1)}, ...), condition=%wide.region_30.31_spmd, body=%wide.region_25.30_spmd.sunk | while | flops 102500352 | bytes 5177615 | solution.py:284
  486.3 2.0 conditional.12
  489.4 2.0 conditional.12
  492.6 2.0 conditional.12
  495.7 2.0 conditional.12
  498.9 2.0 conditional.12
  502.1 2.0 conditional.12
  505.2 2.0 conditional.12
  508.4 2.0 conditional.12
  510.4 3.1 copy.260
  513.6 4.1 copy.196
  517.7 3.9 copy.197
  521.6 50.2 %while.86 = (s32[]{:T(128)}, f32[2,2,256]{2,1,0:T(2,128)S(1)}, f32[2,2,256]{2,1,0:T(2,128)S(1)}, f32[2,2,256,128]{3,2,1,0:T(8,128)S(1)}, s32[16]{0:T(128)S(1)}, ...) while((s32[]{:T(128)}, f32[2,2,256]{2,1,0:T(2,128)S(1)}, ...), condition=%wide.region_36.37_spmd, body=%wide.region_31.36_spmd.sunk | while | flops 102500352 | bytes 5177615 | solution.py:284
  524.0 2.1 conditional.13
  527.3 2.1 conditional.13
  530.5 2.1 conditional.13
  533.8 2.1 conditional.13
  537.1 2.1 conditional.13
  540.3 2.1 conditional.13
  543.6 2.1 conditional.13
  546.9 2.1 conditional.13
  550.1 2.1 conditional.13
  553.4 2.1 conditional.13
  556.7 2.1 conditional.13
  559.9 2.1 conditional.13
  563.2 2.1 conditional.13
  566.5 2.1 conditional.13
  569.7 2.1 conditional.13
  573.1 2.1 fusion.54
  575.7 48.8 %all_to_all.5 = bf16[4,256,2048]{2,1,0:T(8,128)(2,1)} all-to-all(bf16[4,256,2048]{2,1,0:T(8,128)(2,1)S(1)} %broadcast_in_dim.56), channel_id=1, replica_groups=mesh['sp_0'=8,'sp_1'=8,'sp_2'=2,'tp'=4] {'tp'}, dimensions={0} | all-to-all | bytes 8388608 | tf_op jit(solution)/shard_map/all_to_all | solution.py:62
  624.5 4.2 reduce_sum.105
  (447 shorter events, 116.5 us)
Async XLA Ops:
  6.5 456.2 %copy-start = (bf16[256,2048]{1,0:T(8,128)(2,1)S(1)}, bf16[256,2048]{1,0:T(8,128)(2,1)}, u32[]{:S(2)}) copy-start(bf16[256,2048]{1,0:T(8,128)(2,1)} %param.43) | copy-start | bytes 3145732
  6.5 91.5 %all-gather.4.cloned.1.call-start = ((), (), s32[]{:S(2)}) async-start(), calls=%async_computation.1 | async-start | bytes 6340608 | tf_op jit(solution)/shard_map/all_gather | solution.py:23
  10.8 0.6 copy-start.18
  13.7 86.7 %copy-start.8 = (bf16[256,2048]{1,0:T(8,128)(2,1)S(1)}, bf16[256,2048]{1,0:T(8,128)(2,1)}, u32[]{:S(2)}) copy-start(bf16[256,2048]{1,0:T(8,128)(2,1)} %param.35) | copy-start | bytes 3145732
  13.7 86.7 %copy-start.35 = (f32[2048]{0:T(1024)S(1)}, f32[2048]{0:T(1024)}, u32[]{:S(2)}) copy-start(f32[2048]{0:T(1024)} %param.36) | copy-start | bytes 24580
  102.3 4.2 copy-start.36
  104.4 77.1 %copy-start.3 = (bf16[256,256]{0,1:T(8,128)(2,1)}, bf16[256,256]{0,1:T(8,128)(2,1)S(1)}, u32[]{:S(2)}) copy-start(bf16[256,256]{0,1:T(8,128)(2,1)S(1)} %convolution_convert_fusion) | copy-start | bytes 393220
  104.4 50.9 %collective-permute-start.1 = (bf16[256,256]{0,1:T(8,128)(2,1)S(1)}, bf16[256,256]{0,1:T(8,128)(2,1)S(1)}, u32[]{:S(2)}, u32[]{:S(2)}) collective-permute-start(bf16[256,256]{0,1:T(8,128)(2,1)S(1)} %convolution_convert_fusion), channel_id=1, source_target_pairs={{0,4},{4,8},{8,12},{12,16},{16,20},{20,24},{24,28},{28,32},{32,36}... | collective-permute-start | bytes 393224 | tf_op jit(solution)/shard_map/ppermute | solution.py:57
  111.4 6.3 copy-start.9
  111.4 6.3 copy-start.29
  113.5 26.6 %copy-start.14 = (bf16[256,4,32]{0,2,1:T(8,128)(2,1)}, bf16[256,4,32]{0,2,1:T(8,128)(2,1)S(1)}, u32[]{:S(2)}) copy-start(bf16[256,4,32]{0,2,1:T(8,128)(2,1)S(1)} %get-tuple-element.1297) | copy-start | bytes 196612
  113.5 26.6 %copy-start.16 = (bf16[256,4,32]{0,2,1:T(8,128)(2,1)}, bf16[256,4,32]{0,2,1:T(8,128)(2,1)S(1)}, u32[]{:S(2)}) copy-start(bf16[256,4,32]{0,2,1:T(8,128)(2,1)S(1)} %get-tuple-element.1298) | copy-start | bytes 196612
  113.5 72.2 %copy-start.1 = (bf16[256,4,64]{0,2,1:T(8,128)(2,1)}, bf16[256,4,64]{0,2,1:T(8,128)(2,1)S(1)}, u32[]{:S(2)}) copy-start(bf16[256,4,64]{0,2,1:T(8,128)(2,1)S(1)} %pad_maximum_fusion.7) | copy-start | bytes 393220
  113.5 27.5 %collective-permute-start = (bf16[256,256]{0,1:T(8,128)(2,1)S(1)}, bf16[256,256]{0,1:T(8,128)(2,1)S(1)}, u32[]{:S(2)}, u32[]{:S(2)}) collective-permute-start(bf16[256,256]{0,1:T(8,128)(2,1)S(1)} %bitcast.526), channel_id=1, source_target_pairs={{0,4},{4,8},{8,12},{12,16},{16,20},{20,24},{24,28},{28,32},{32,36}... | collective-permute-start | bytes 393224 | tf_op jit(solution)/shard_map/ppermute | solution.py:57
  118.3 16.0 %copy-start.11 = (f32[2,128,2,128]{1,3,2,0:T(8,128)}, f32[2,128,2,128]{1,3,2,0:T(8,128)S(1)}, u32[]{:S(2)}) copy-start(f32[2,128,2,128]{1,3,2,0:T(8,128)S(1)} %copy.179) | copy-start | bytes 786436
  134.3 5.8 copy-start.19
  140.1 11.7 %copy-start.6 = (f32[4,2,64,128]{3,2,0,1:T(8,128)}, f32[4,2,64,128]{3,2,0,1:T(8,128)S(1)}, u32[]{:S(2)}) copy-start(f32[4,2,64,128]{3,2,0,1:T(8,128)S(1)} %get-tuple-element.1863) | copy-start | bytes 786436
  141.0 10.7 %collective-permute-start.2 = (bf16[512,256]{0,1:T(8,128)(2,1)S(1)}, bf16[512,256]{0,1:T(8,128)(2,1)S(1)}, u32[]{:S(2)}, u32[]{:S(2)}) collective-permute-start(bf16[512,256]{0,1:T(8,128)(2,1)S(1)} %pad_maximum_fusion.4), channel_id=1, source_target_pairs={{0,8},{4,12},{8,16},{12,20},{16,24},{20,28},{24,32},{28,36},{32,40... | collective-permute-start | bytes 786440 | tf_op jit(solution)/shard_map/ppermute | solution.py:57
  151.8 33.9 %collective-permute-start.4 = (bf16[1024,256]{0,1:T(8,128)(2,1)S(1)}, bf16[1024,256]{0,1:T(8,128)(2,1)S(1)}, u32[]{:S(2)}, u32[]{:S(2)}) collective-permute-start(bf16[1024,256]{0,1:T(8,128)(2,1)S(1)} %pad_maximum_fusion.2), channel_id=1, source_target_pairs={{0,16},{4,20},{8,24},{12,28},{16,32},{20,36},{24,40},{28,44},{32,4... | collective-permute-start | bytes 1572872 | tf_op jit(solution)/shard_map/ppermute | solution.py:57
  155.3 26.2 %collective-permute-start.3 = (bf16[512,256]{0,1:T(8,128)(2,1)S(1)}, bf16[512,256]{0,1:T(8,128)(2,1)S(1)}, u32[]{:S(2)}, u32[]{:S(2)}) collective-permute-start(bf16[512,256]{0,1:T(8,128)(2,1)S(1)} %pad_maximum_fusion.5), channel_id=1, source_target_pairs={{0,8},{4,12},{8,16},{12,20},{16,24},{20,28},{24,32},{28,36},{32,40... | collective-permute-start | bytes 786440 | tf_op jit(solution)/shard_map/ppermute | solution.py:57
  181.5 22.4 %copy-start.4 = (bf16[256,256]{0,1:T(8,128)(2,1)S(1)}, bf16[256,256]{0,1:T(8,128)(2,1)}, u32[]{:S(2)}) copy-start(bf16[256,256]{0,1:T(8,128)(2,1)} %copy-done.3) | copy-start | bytes 393220
  181.5 105.5 %collective-permute-start.5 = (bf16[1024,256]{0,1:T(8,128)(2,1)S(1)}, bf16[1024,256]{0,1:T(8,128)(2,1)S(1)}, u32[]{:S(2)}, u32[]{:S(2)}) collective-permute-start(bf16[1024,256]{0,1:T(8,128)(2,1)S(1)} %pad_maximum_fusion.3), channel_id=1, source_target_pairs={{0,16},{4,20},{8,24},{12,28},{16,32},{20,36},{24,40},{28,44},{32,4... | collective-permute-start | bytes 1572872 | tf_op jit(solution)/shard_map/ppermute | solution.py:57
  186.8 105.5 %collective-permute-start.6 = (bf16[2048,256]{0,1:T(8,128)(2,1)}, bf16[2048,256]{0,1:T(8,128)(2,1)}, u32[]{:S(2)}, u32[]{:S(2)}) collective-permute-start(bf16[2048,256]{0,1:T(8,128)(2,1)} %pad_maximum_fusion), channel_id=1, source_target_pairs={{0,32},{4,36},{8,40},{12,44},{16,48},{20,52},{24,56},{28,60},{32,6... | collective-permute-start | bytes 3145736 | tf_op jit(solution)/shard_map/ppermute | solution.py:57
  288.1 54.4 %collective-permute-start.7 = (bf16[2048,256]{0,1:T(8,128)(2,1)}, bf16[2048,256]{0,1:T(8,128)(2,1)}, u32[]{:S(2)}, u32[]{:S(2)}) collective-permute-start(bf16[2048,256]{0,1:T(8,128)(2,1)} %pad_maximum_fusion.1), channel_id=1, source_target_pairs={{0,32},{4,36},{8,40},{12,44},{16,48},{20,52},{24,56},{28,60},{32,6... | collective-permute-start | bytes 3145736 | tf_op jit(solution)/shard_map/ppermute | solution.py:57
  292.3 4.8 copy-start.2
  297.1 50.1 %copy-start.5 = (bf16[256,256]{0,1:T(8,128)(2,1)S(1)}, bf16[256,256]{0,1:T(8,128)(2,1)}, u32[]{:S(2)}) copy-start(bf16[256,256]{0,1:T(8,128)(2,1)} %copy-done.3) | copy-start | bytes 393220
  297.8 55.8 %copy-start.15 = (bf16[256,4,32]{0,2,1:T(8,128)(2,1)S(1)}, bf16[256,4,32]{0,2,1:T(8,128)(2,1)}, u32[]{:S(2)}) copy-start(bf16[256,4,32]{0,2,1:T(8,128)(2,1)} %copy-done.14) | copy-start | bytes 196612
  297.8 55.8 %copy-start.17 = (bf16[256,4,32]{0,2,1:T(8,128)(2,1)S(1)}, bf16[256,4,32]{0,2,1:T(8,128)(2,1)}, u32[]{:S(2)}) copy-start(bf16[256,4,32]{0,2,1:T(8,128)(2,1)} %copy-done.16) | copy-start | bytes 196612
  297.8 55.9 %copy-start.20 = (f32[2,128]{1,0:T(2,128)S(1)}, f32[2,128]{1,0:T(2,128)}, u32[]{:S(2)}) copy-start(f32[2,128]{1,0:T(2,128)} %broadcast_multiply_fusion) | copy-start | bytes 3076
  297.8 55.9 %copy-start.21 = (f32[2,128]{1,0:T(2,128)S(1)}, f32[2,128]{1,0:T(2,128)}, u32[]{:S(2)}) copy-start(f32[2,128]{1,0:T(2,128)} %convert_bitcast_fusion.10) | copy-start | bytes 3076
  344.8 44.5 %copy-start.22 = (f32[2,128]{1,0:T(2,128)S(1)}, f32[2,128]{1,0:T(2,128)}, u32[]{:S(2)}) copy-start(f32[2,128]{1,0:T(2,128)} %get-tuple-element.1314) | copy-start | bytes 3076
  344.8 44.5 %copy-start.23 = (f32[2,128]{1,0:T(2,128)S(1)}, f32[2,128]{1,0:T(2,128)}, u32[]{:S(2)}) copy-start(f32[2,128]{1,0:T(2,128)} %get-tuple-element.1315) | copy-start | bytes 3076
  344.8 44.5 %copy-start.24 = (f32[2,128]{1,0:T(2,128)S(1)}, f32[2,128]{1,0:T(2,128)}, u32[]{:S(2)}) copy-start(f32[2,128]{1,0:T(2,128)} %get-tuple-element.1316) | copy-start | bytes 3076
  344.8 44.5 %copy-start.25 = (f32[2,128]{1,0:T(2,128)S(1)}, f32[2,128]{1,0:T(2,128)}, u32[]{:S(2)}) copy-start(f32[2,128]{1,0:T(2,128)} %get-tuple-element.1317) | copy-start | bytes 3076
  344.8 44.5 %copy-start.26 = (f32[2,128]{1,0:T(2,128)S(1)}, f32[2,128]{1,0:T(2,128)}, u32[]{:S(2)}) copy-start(f32[2,128]{1,0:T(2,128)} %get-tuple-element.1318) | copy-start | bytes 3076
  344.8 44.5 %copy-start.27 = (f32[2,128]{1,0:T(2,128)S(1)}, f32[2,128]{1,0:T(2,128)}, u32[]{:S(2)}) copy-start(f32[2,128]{1,0:T(2,128)} %get-tuple-element.1319) | copy-start | bytes 3076
  344.9 44.5 %copy-start.28 = (f32[2,128]{1,0:T(2,128)S(1)}, f32[2,128]{1,0:T(2,128)}, u32[]{:S(2)}) copy-start(f32[2,128]{1,0:T(2,128)} %get-tuple-element.1320) | copy-start | bytes 3076
  344.9 116.3 %copy-start.7 = (f32[4,2,64,128]{3,2,0,1:T(8,128)S(1)}, f32[4,2,64,128]{3,2,0,1:T(8,128)}, u32[]{:S(2)}) copy-start(f32[4,2,64,128]{3,2,0,1:T(8,128)} %copy-done.6) | copy-start | bytes 786436
  344.9 116.3 %copy-start.12 = (f32[2,128,2,128]{1,3,2,0:T(8,128)S(1)}, f32[2,128,2,128]{1,3,2,0:T(8,128)}, u32[]{:S(2)}) copy-start(f32[2,128,2,128]{1,3,2,0:T(8,128)} %copy-done.11) | copy-start | bytes 786436
  344.9 116.3 %copy-start.13 = (f32[2,256,128]{1,2,0:T(8,128)S(1)}, f32[2,256,128]{1,2,0:T(8,128)}, u32[]{:S(2)}) copy-start(f32[2,256,128]{1,2,0:T(8,128)} %copy.183) | copy-start | bytes 786436
  344.9 116.3 %copy-start.30 = (f32[2,128]{1,0:T(2,128)S(1)}, f32[2,128]{1,0:T(2,128)}, u32[]{:S(2)}) copy-start(f32[2,128]{1,0:T(2,128)} %get-tuple-element.1277) | copy-start | bytes 3076
  344.9 116.3 %copy-start.31 = (f32[2,128]{1,0:T(2,128)S(1)}, f32[2,128]{1,0:T(2,128)}, u32[]{:S(2)}) copy-start(f32[2,128]{1,0:T(2,128)} %get-tuple-element.1278) | copy-start | bytes 3076
  344.9 116.3 %copy-start.37 = (f32[2,128]{1,0:T(2,128)S(1)}, f32[2,128]{1,0:T(2,128)}, u32[]{:S(2)}) copy-start(f32[2,128]{1,0:T(2,128)} %multiply_bitcast_fusion) | copy-start | bytes 3076
  347.9 162.6 %collective-permute-start.9 = (bf16[4096,256]{0,1:T(8,128)(2,1)}, bf16[4096,256]{0,1:T(8,128)(2,1)}, u32[]{:S(2)}, u32[]{:S(2)}) collective-permute-start(bf16[4096,256]{0,1:T(8,128)(2,1)} %constant_dynamic-update-slice_fusion.11), channel_id=1, source_target_pairs={{0,64},{4,68},{8,72},{12,76},{16,80},{20,84},{24,88},{28,92},{32,9... | collective-permute-start | bytes 6291464 | tf_op jit(solution)/shard_map/ppermute | solution.py:57
  349.8 163.8 %collective-permute-start.8 = (bf16[4096,256]{0,1:T(8,128)(2,1)}, bf16[4096,256]{0,1:T(8,128)(2,1)}, u32[]{:S(2)}, u32[]{:S(2)}) collective-permute-start(bf16[4096,256]{0,1:T(8,128)(2,1)} %constant_dynamic-update-slice_fusion.6), channel_id=1, source_target_pairs={{0,64},{4,68},{8,72},{12,76},{16,80},{20,84},{24,88},{28,92},{32,9... | collective-permute-start | bytes 6291464 | tf_op jit(solution)/shard_map/ppermute | solution.py:57
  389.7 73.0 %copy-start.32 = (f32[128]{0:T(128)S(1)}, f32[128]{0:T(128)}, u32[]{:S(2)}) copy-start(f32[128]{0:T(128)} %param.47) | copy-start | bytes 1540
  521.6 50.5 %copy-start.34 = (f32[2]{0:T(128)S(1)}, f32[2]{0:T(128)}, u32[]{:S(2)}) copy-start(f32[2]{0:T(128)} %param.49) | copy-start | bytes 28
  521.6 50.6 %copy-start.33 = (f32[128]{0:T(128)S(1)}, f32[128]{0:T(128)}, u32[]{:S(2)}) copy-start(f32[128]{0:T(128)} %param.48) | copy-start | bytes 1540
  571.8 1.2 copy-start.10
Sparse Core Ops, SparseCore 0:
  11.6 86.4 all-gather.3
where the time goes:
time: 638 us; the launch traced here: 636 us
  waiting for transfers between devices  236 us (37%)
  blocking collectives  185 us (29%)
  local copies, waits for them, and re-layouts  76.2 us (12%)
  matrix products  48.7 us (8%)
  starting transfers between devices  35.4 us (6%)
  loops' own time  20.1 us (3%)
  other arithmetic  19.5 us (3%)
  between operations  14.3 us (2%)
    ppermute x10, waiting for transfers between devices, from_behind(): return lax.ppermute(block, axis, route)  152 us
    all_gather x6, blocking collectives, entering(): lax.all_gather(part.astype(kind), axis)  136 us
    all_gather x1, waiting for transfers between devices, sent_together(): result = lax.all_gather(both, axis, axis=dim, tiled=True)  84.1 us
    all_to_all x1, blocking collectives, copy_for_each(): lax.all_to_all(jnp.broadcast_to(array[None], (count, *array.shape)), axis...  48.8 us
    dynamic_slice x59, local copies, waits for them, and re-layouts, per_device(): lax.scan(absorb_piece, online, (jnp.arange(stride, dtype=jnp.int32), far_...  39.8 us
    ppermute x10, starting transfers between devices, from_behind(): return lax.ppermute(block, axis, route)  35.4 us
    another operation x4, loops' own time, per_device(): lax.scan(absorb_piece, online, (jnp.arange(stride, dtype=jnp.int32), far_...  18.3 us
    dot_general x31, matrix products, absorb(): jnp.einsum('hcqk,khe->hcqe', expo_vals.astype(jnp.bfloat16), value_rows,...  15.2 us
  transfers between devices with their start and end apart: 11, of which 5 were waited for; matrix products, arithmetic and copies ran while one was open for 11% of the time, Pallas kernels for 0%

commit v1 on v0

v1 whole, which is shorter than its diff:
```python
import functools

import jax
import jax.numpy as jnp
from jax import lax
from jax.experimental import pallas as pl
from jax.experimental.pallas import tpu as pltpu
from jax.sharding import Mesh
from jax.sharding import PartitionSpec as P

HEAD = 128
PAIR = 64
BLOCK = 64
SP = ("sp_0", "sp_1", "sp_2")
NZ, NY, NX = 8, 8, 4
HALF = NY // 2
TOK = 256
QUART = TOK // NX
ST_ROWS = 144
RECUR_EPSILON = 1e-06
ATTEND_EPSILON = 1e-05
ROTARY_BASE = 10000.0
SCORE_LOG2 = PAIR ** (-0.5) * 1.4426950408889634
F32, BF16 = jnp.float32, jnp.bfloat16
MESH_ID = pl.DeviceIdType.MESH
NT = (((1,), (1,)), ((), ()))


def remote(src, dst, send, recv, where):
    return pltpu.make_async_remote_copy(
        src_ref=src, dst_ref=dst, send_sem=send, recv_sem=recv, device_id=where, device_id_type=MESH_ID
    )


def greet(places):
    barrier = pltpu.get_barrier_semaphore()
    for place in places:
        pl.semaphore_signal(barrier, inc=1, device_id=place, device_id_type=MESH_ID)
    pl.semaphore_wait(barrier, len(places))


def where_am_i():
    return (lax.axis_index("sp_0"), lax.axis_index("sp_1"), lax.axis_index("sp_2"), lax.axis_index("tp"))


def partner_row(z):
    return jnp.where(z % 2 == 1, (z + 1) % NZ, (z + NZ - 1) % NZ)


class Ring:
    def __init__(self, y, c, first, piece, sems):
        self.y, self.c, self.first, self.piece = y, c, first, piece
        self.sr, self.rr, self.sl, self.rl, self.sp, self.rp = sems
        self.right = {"sp_1": (y + 1) % NY}
        self.left = {"sp_1": (y + NY - 1) % NY}
        self.other = {"sp_2": 1 - c}

    def source(self, offset, h):
        if offset == 0:
            return self.first(h)
        return self.piece((self.y + offset + NY) % NY, self.c, h)

    def to_right(self, k, h):
        origin = (self.y - (k - 1) + NY) % NY
        i = 2 * (k - 1) + h
        return remote(
            self.source(1 - k, h), self.piece(origin, self.c, h), self.sr.at[i], self.rr.at[i], self.right
        )

    def to_left(self, k, h):
        origin = (self.y + (k - 1)) % NY
        i = 2 * (k - 1) + h
        return remote(
            self.source(k - 1, h), self.piece(origin, self.c, h), self.sl.at[i], self.rl.at[i], self.left
        )

    def to_other(self, offset, h):
        i = 2 * (offset % NY) + h
        origin = (self.y + offset + NY) % NY
        return remote(
            self.source(offset, h), self.piece(origin, self.c, h), self.sp.at[i], self.rp.at[i], self.other
        )

    def from_side(self, offset, h, sems, i):
        ref = self.piece((self.y + offset + NY) % NY, self.c, h)
        return remote(ref, ref, self.sr.at[0], sems.at[i], self.right)

    def goes_right(self, k, h):
        return k < HALF or (k == HALF and h == 0)

    def goes_left(self, k, h):
        return k < HALF or (k == HALF and h == 1)

    def begin(self):
        for h in range(2):
            self.to_right(1, h).start()
            self.to_left(1, h).start()
        for h in range(2):
            self.to_other(0, h).start()

    def step(self, k, h):
        if self.goes_right(k, h):
            self.from_side(-k, h, self.rr, 2 * (k - 1) + h).wait_recv()
            if self.goes_right(k + 1, h):
                self.to_right(k + 1, h).start()
            self.to_other(-k, h).start()
        if self.goes_left(k, h):
            self.from_side(k, h, self.rl, 2 * (k - 1) + h).wait_recv()
            if self.goes_left(k + 1, h):
                self.to_left(k + 1, h).start()
            self.to_other(k, h).start()

    def wait_other(self, offset, h):
        ref = self.piece((self.y + offset + NY) % NY, 1 - self.c, h)
        remote(ref, ref, self.sp.at[0], self.rp.at[2 * (offset % NY) + h], self.other).wait_recv()

    def finish(self):
        for k in range(1, HALF + 1):
            for h in range(2):
                if self.goes_right(k, h):
                    self.to_right(k, h).wait_send()
                if self.goes_left(k, h):
                    self.to_left(k, h).wait_send()
        for offset in range(NY):
            for h in range(2):
                self.to_other(offset, h).wait_send()


def ring_sems():
    return [
        pltpu.SemaphoreType.DMA((2 * HALF,)),
        pltpu.SemaphoreType.DMA((2 * HALF,)),
        pltpu.SemaphoreType.DMA((2 * HALF,)),
        pltpu.SemaphoreType.DMA((2 * HALF,)),
        pltpu.SemaphoreType.DMA((2 * NY,)),
        pltpu.SemaphoreType.DMA((2 * NY,)),
    ]


def project_kernel(
    x_ref, w_ref, ds_ref, gain_ref, cos_ref, sin_ref,
    rec_ref, q_ref, kv_ref, dso_ref,
    xp, xn, wbuf, dsp,
    t1s, t1r, t2s, t2r, dss, dsr, w1s, w1r, *sems,
):
    z, y, c, x = where_am_i()
    zp = partner_row(z)
    row = (z + 1) % 2
    right, left = (x + 1) % NX, (x + NX - 1) % NX
    greet(
        [{"sp_0": (z + d) % NZ} for d in range(1, NZ)]
        + [{"tp": right}, {"tp": left}]
        + [{"sp_1": (y + 1) % NY}, {"sp_1": (y + NY - 1) % NY}, {"sp_2": 1 - c}]
    )
    across = remote(x_ref.at[x], xp.at[x], t1s.at[0], t1r.at[0], {"sp_0": zp})
    spread = []
    for d in (1, 7, 2, 6, 3, 5, 4):
        there = (z + d) % NZ
        spread.append(
            remote(
                w_ref.at[(there + 1) % 2], wbuf.at[z, y, c], w1s.at[d - 1], w1r.at[d - 1], {"sp_0": there}
            )
        )
    for copy in spread:
        copy.start()
    across.start()
    shifts = remote(ds_ref, dsp, dss.at[0], dsr.at[0], {"sp_0": zp})
    shifts.start()
    wbuf[z, y, c] = w_ref[row]

    def normed(values):
        values = values.astype(F32)
        mean_sq = jnp.mean(values * values, axis=-1, keepdims=True)
        return (values * lax.rsqrt(mean_sq + RECUR_EPSILON) * gain_ref[...]).astype(BF16)

    for d in range(1, NZ):
        ref = wbuf.at[(z + NZ - d) % NZ, y, c]
        remote(ref, ref, w1s.at[d - 1], w1r.at[d - 1], {"sp_0": zp}).wait_recv()
    piece = lambda yo, stream, h: wbuf.at[pl.ds(h * (NZ // 2), NZ // 2), yo, stream]
    ring = Ring(y, c, lambda h: piece(y, c, h), piece, sems)
    ring.begin()
    across.wait_recv()
    to_right = remote(xp.at[x], xp.at[x], t2s.at[0], t2r.at[0], {"tp": right})
    to_left = remote(xp.at[x], xp.at[x], t2s.at[1], t2r.at[1], {"tp": left})
    to_right.start()
    to_left.start()
    for i in range(NX):
        xn[row, pl.ds(i * QUART, QUART)] = normed(x_ref[i])
    ring.step(1, 0)
    ring.step(1, 1)
    half = QUART // 2
    mine_l, mine_r = xp.at[left], xp.at[right]
    remote(mine_l, mine_l, t2s.at[0], t2r.at[0], {"tp": right}).wait_recv()
    far_l = xp.at[left, pl.ds(0, half)]
    on_right = remote(far_l, far_l, t2s.at[2], t2r.at[2], {"tp": right})
    on_right.start()
    remote(mine_r, mine_r, t2s.at[1], t2r.at[1], {"tp": left}).wait_recv()
    far_r = xp.at[right, pl.ds(half, half)]
    on_left = remote(far_r, far_r, t2s.at[3], t2r.at[3], {"tp": left})
    on_left.start()
    for k in range(2, HALF + 1):
        for h in range(2):
            ring.step(k, h)
    opposite = (x + 2) % NX
    got_a = xp.at[opposite, pl.ds(0, half)]
    got_b = xp.at[opposite, pl.ds(half, half)]
    remote(got_a, got_a, t2s.at[2], t2r.at[2], {"tp": right}).wait_recv()
    remote(got_b, got_b, t2s.at[3], t2r.at[3], {"tp": left}).wait_recv()
    for i in range(NX):
        xn[1 - row, pl.ds(i * QUART, QUART)] = normed(xp[i])
    shifts.wait_recv()
    dso_ref[pl.ds(row, 1)] = ds_ref[pl.ds(row, 1)]
    dso_ref[pl.ds(1 - row, 1)] = dsp[pl.ds(row, 1)]
    for offset in range(NY):
        for h in range(2):
            ring.wait_other(offset, h)

    lane = lax.broadcasted_iota(jnp.int32, (TOK, HEAD), 1)
    first = (lane % PAIR) < (PAIR // 2)

    def turned(values, kind):
        swapped = jnp.where(
            first, pltpu.roll(values, HEAD - PAIR // 2, 1), pltpu.roll(values, PAIR // 2, 1)
        )
        return (values * cos_ref[kind] + swapped * sin_ref[kind]).astype(BF16)

    for part in range(3):
        weight = wbuf[:, :, :, :, pl.ds(part * 256, 256)].reshape(NZ * NY * 2 * 16, 256)
        for kind in range(2):
            out = jnp.dot(xn[kind], weight, preferred_element_type=F32)
            one, two = out[:, :HEAD], out[:, HEAD:]
            if part == 0:
                rec_ref[0, kind] = one.astype(BF16)
                rec_ref[1, kind] = two.astype(BF16)
            elif part == 1:
                rec_ref[2, kind] = one.astype(BF16)
                kv_ref[kind, :, pl.ds(HEAD, HEAD)] = two.astype(BF16)
            else:
                q_ref[kind] = turned(one, kind)
                kv_ref[kind, :, pl.ds(0, HEAD)] = turned(two, kind)
    ring.finish()
    for copy in spread:
        copy.wait_send()
    for copy in (across, shifts, to_right, to_left, on_right, on_left):
        copy.wait_send()


def mix_kernel(
    rec_ref, q_ref, kv_ref, ds_ref, fg_ref, lam_ref, rgain_ref, again_ref,
    mix_ref,
    kvbuf, stbuf, q2, m_s, l_s, acc, local, qdec, *sems,
):
    z, y, c, x = where_am_i()
    row = (z + 1) % 2
    linked = jnp.logical_and(z != 0, z != NZ - 1)
    greet([{"sp_1": (y + 1) % NY}, {"sp_1": (y + NY - 1) % NY}, {"sp_2": 1 - c}])
    kv_ring = Ring(
        y, c, lambda h: kv_ref.at[h], lambda yo, stream, h: kvbuf.at[yo, h, stream], sems[:6]
    )
    st_ring = Ring(
        y, c, lambda h: stbuf.at[y, c, h], lambda yo, stream, h: stbuf.at[yo, stream, h], sems[6:]
    )
    kv_ring.begin()
    kvbuf[y, 0, c] = kv_ref[0]
    kvbuf[y, 1, c] = kv_ref[1]

    causal = lax.broadcasted_iota(jnp.int32, (BLOCK, BLOCK), 0) >= lax.broadcasted_iota(
        jnp.int32, (BLOCK, BLOCK), 1
    )
    tril = jnp.where(causal, 1.0, 0.0).astype(F32)
    gap = fg_ref[pl.ds(row, 1)]

    def segment(kind):
        shift = jnp.broadcast_to(ds_ref[pl.ds(kind, 1)], (HEAD, TOK)).T
        state = jnp.zeros((HEAD, HEAD), F32)
        total = jnp.zeros((1, HEAD), F32)
        for b in range(TOK // BLOCK):
            rows = pl.ds(b * BLOCK, BLOCK)
            forget = rec_ref[1, kind, rows].astype(F32)
            query = rec_ref[0, kind, rows].astype(F32)
            value = rec_ref[2, kind, rows]
            gate = gap * (1.0 / (1.0 + jnp.exp(forget)))
            decay = jnp.log1p(-gate) + shift[b * BLOCK : (b + 1) * BLOCK]
            cum = jnp.dot(tril, decay, precision=lax.Precision.HIGHEST, preferred_element_type=F32)
            end = cum[BLOCK - 1 :, :]
            q_dec = query * jnp.exp(cum)
            qdec[kind, rows] = (q_dec * jnp.exp(total)).astype(BF16)
            q_dec = q_dec.astype(BF16)
            k_grow = (gate * jnp.exp(-cum)).astype(BF16)
            scores = lax.dot_general(q_dec, k_grow, NT, preferred_element_type=F32)
            scores = jnp.where(causal, scores, 0.0).astype(BF16)
            out = jnp.dot(scores, value, preferred_element_type=F32)
            if b > 0:
                out = out + lax.dot_general(q_dec, state.astype(BF16), NT, preferred_element_type=F32)
            local[kind, rows] = out
            k_end = (gate * jnp.exp(end - cum)).astype(BF16)
            fresh = jnp.dot(value.astype(F32).T.astype(BF16), k_end, preferred_element_type=F32)
            state = state * jnp.exp(end) + fresh
            total = total + end
        stbuf[y, c, kind, pl.ds(0, HEAD)] = state.astype(BF16)
        high = total.astype(BF16)
        rest = total - high.astype(F32)
        middle = rest.astype(BF16)
        low = (rest - middle.astype(F32)).astype(BF16)
        index = lax.broadcasted_iota(jnp.int32, (ST_ROWS - HEAD, HEAD), 0)
        stack = jnp.where(
            index == 0, high.astype(F32), jnp.where(index == 1, middle.astype(F32), low.astype(F32))
        )
        stbuf[y, c, kind, pl.ds(HEAD, ST_ROWS - HEAD)] = stack.astype(BF16)

    segment(0)
    segment(1)
    st_ring.begin()

    lane = lax.broadcasted_iota(jnp.int32, (TOK, HEAD), 1)
    for kind in range(2):
        q_all = q_ref[kind].astype(F32)
        q2[kind, pl.ds(0, TOK)] = jnp.where(lane < PAIR, q_all, 0.0).astype(BF16)
        q2[kind, pl.ds(TOK, TOK)] = jnp.where(lane >= PAIR, q_all, 0.0).astype(BF16)

    def keys_values(yo, kind):
        both = kvbuf[yo, kind].reshape(2 * TOK, 2 * HEAD)
        return both[:, :HEAD], both[:, HEAD:]

    for h in range(2):
        kv_ring.wait_other(0, h)

    def own(kind, carry):
        keys, values = keys_values(y, kind)
        for part in range(2):
            rows = pl.ds(part * TOK, TOK)
            scores = lax.dot_general(q2[kind, rows], keys, NT, preferred_element_type=F32)
            seen = lax.broadcasted_iota(jnp.int32, (TOK, 2 * TOK), 1) <= (
                lax.broadcasted_iota(jnp.int32, (TOK, 2 * TOK), 0) + c * TOK
            )
            scores = jnp.where(seen, scores, -jnp.inf)
            best = jnp.max(scores, axis=-1, keepdims=True)
            expo = jnp.exp2((scores - best) * SCORE_LOG2)
            m_s[kind, rows] = jnp.broadcast_to(best, (TOK, HEAD))
            l_s[kind, rows] = jnp.broadcast_to(jnp.sum(expo, axis=-1, keepdims=True), (TOK, HEAD))
            acc[kind, rows] = jnp.dot(expo.astype(BF16), values, preferred_element_type=F32)
        return carry

    lax.fori_loop(0, 2, own, 0)

    def absorb(yo, q_kind, kv_kind):
        keys, values = keys_values(yo, kv_kind)
        for part in range(2):
            rows = pl.ds(part * TOK, TOK)
            scores = lax.dot_general(q2[q_kind, rows], keys, NT, preferred_element_type=F32)
            old = m_s[q_kind, rows]
            best = jnp.maximum(old, jnp.max(scores, axis=-1, keepdims=True))
            scale = jnp.exp2((old - best) * SCORE_LOG2)
            expo = jnp.exp2((scores - best[:, :1]) * SCORE_LOG2)
            m_s[q_kind, rows] = best
            l_s[q_kind, rows] = l_s[q_kind, rows] * scale + jnp.sum(expo, axis=-1, keepdims=True)
            acc[q_kind, rows] = acc[q_kind, rows] * scale + jnp.dot(
                expo.astype(BF16), values, preferred_element_type=F32
            )

    def process(offsets):
        for offset in offsets:
            for h in range(2):
                if offset:
                    kv_ring.wait_other(offset, h)

        def unit(i, carry):
            which = i // 3
            kind_at = i % 3
            offset = jnp.where(which == 0, offsets[0], offsets[-1])
            yo = (y + offset + NY) % NY
            q_kind = jnp.where(kind_at == 0, 0, 1)
            kv_kind = jnp.where(kind_at == 2, 1, 0)
            wanted = jnp.where(kind_at == 1, linked.astype(jnp.int32), (yo < y).astype(jnp.int32))

            @pl.when(wanted == 1)
            def _():
                absorb(yo, q_kind, kv_kind)

            return carry

        lax.fori_loop(0, 3 * len(offsets), unit, 0)

    for k in range(1, HALF + 1):
        for h in range(2):
            kv_ring.step(k, h)
        if k == 1:
            process((0,))
        else:
            process((1 - k, k - 1))
        for h in range(2):
            st_ring.step(k, h)
    process((HALF,))
    for offset in range(NY):
        for h in range(2):
            st_ring.wait_other(offset, h)

    me = 2 * y + c

    def pass_on(kind, s, state):
        yo, stream = s // 2, s % 2
        tail = stbuf[yo, stream, kind, pl.ds(HEAD, ST_ROWS - HEAD)].astype(F32)
        total = tail[0:1] + tail[1:2] + tail[2:3]
        return state * jnp.exp(total) + stbuf[yo, stream, kind, pl.ds(0, HEAD)].astype(F32)

    nothing = jnp.zeros((HEAD, HEAD), F32)
    into_low = lax.fori_loop(0, me, functools.partial(pass_on, 0), nothing)
    all_low = lax.fori_loop(me, 2 * NY, functools.partial(pass_on, 0), into_low)
    all_low = all_low * jnp.where(linked, 1.0, 0.0)
    into_high = lax.fori_loop(0, me, functools.partial(pass_on, 1), all_low)
    lam = lam_ref[row]
    for kind in range(2):
        state = (into_low if kind == 0 else into_high).astype(BF16)
        raw = local[kind] + lax.dot_general(qdec[kind], state, NT, preferred_element_type=F32)
        mean_sq = jnp.mean(raw * raw, axis=-1, keepdims=True)
        mix_ref[kind, :, pl.ds(0, HEAD)] = (
            raw * lax.rsqrt(mean_sq + RECUR_EPSILON) * rgain_ref[...]
        ).astype(BF16)
        raw = acc[kind, pl.ds(0, TOK)] / l_s[kind, pl.ds(0, TOK)] - lam * (
            acc[kind, pl.ds(TOK, TOK)] / l_s[kind, pl.ds(TOK, TOK)]
        )
        mean_sq = jnp.mean(raw * raw, axis=-1, keepdims=True)
        mix_ref[kind, :, pl.ds(HEAD, HEAD)] = (
            raw * lax.rsqrt(mean_sq + ATTEND_EPSILON) * again_ref[...]
        ).astype(BF16)
    kv_ring.finish()
    st_ring.finish()


def output_kernel(
    mix_ref, wr_ref, wa_ref, out_ref,
    other, part, relay, got,
    ms, mr, s_sem, r_sem, g_send, g_recv,
):
    z, y, c, x = where_am_i()
    row = (z + 1) % 2
    right, left, far = (x + 1) % NX, (x + NX - 1) % NX, (x + 2) % NX
    to_r, to_l = {"tp": right}, {"tp": left}
    zp = {"sp_0": partner_row(z)}
    greet([to_r, to_l, zp])
    swap = remote(mix_ref.at[1 - row], other, ms.at[0], mr.at[0], zp)
    swap.start()
    swap.wait_recv()
    rows_own = pl.ds(row * HEAD, HEAD)
    rows_other = pl.ds((1 - row) * HEAD, HEAD)
    own = mix_ref[row]
    theirs = other[...]
    width = 512
    for j in range(2048 // width):
        cols = pl.ds(j * width, width)
        total = jnp.dot(own[:, :HEAD], wr_ref[rows_own, cols], preferred_element_type=F32)
        total += jnp.dot(own[:, HEAD:], wa_ref[rows_own, cols], preferred_element_type=F32)
        total += jnp.dot(theirs[:, :HEAD], wr_ref[rows_other, cols], preferred_element_type=F32)
        total += jnp.dot(theirs[:, HEAD:], wa_ref[rows_other, cols], preferred_element_type=F32)
        total = total.astype(BF16)
        for i in range(NX):
            part[i, :, cols] = total[i * QUART : (i + 1) * QUART]
    half = QUART // 2
    top, low = pl.ds(0, half), pl.ds(half, half)
    sends = [
        remote(part.at[far, top], relay.at[0], s_sem.at[0], r_sem.at[0], to_r),
        remote(part.at[far, low], relay.at[1], s_sem.at[1], r_sem.at[1], to_l),
        remote(part.at[right], got.at[0], s_sem.at[2], r_sem.at[2], to_r),
        remote(part.at[left], got.at[1], s_sem.at[3], r_sem.at[3], to_l),
    ]
    for copy in sends:
        copy.start()
    sends[0].wait_recv()
    on_r = remote(relay.at[0], got.at[2, top], s_sem.at[4], r_sem.at[4], to_r)
    on_r.start()
    sends[1].wait_recv()
    on_l = remote(relay.at[1], got.at[2, low], s_sem.at[5], r_sem.at[5], to_l)
    on_l.start()
    sends[2].wait_recv()
    sends[3].wait_recv()
    on_r.wait_recv()
    on_l.wait_recv()
    summed = part[x].astype(F32) + got[0].astype(F32) + got[1].astype(F32) + got[2].astype(F32)
    out_ref[x] = summed.astype(BF16)
    g_r = remote(out_ref.at[x], out_ref.at[x], g_send.at[0], g_recv.at[0], to_r)
    g_l = remote(out_ref.at[x], out_ref.at[x], g_send.at[1], g_recv.at[1], to_l)
    g_r.start()
    g_l.start()
    from_l, from_r = out_ref.at[left], out_ref.at[right]
    remote(from_l, from_l, g_send.at[0], g_recv.at[0], to_r).wait_recv()
    pass_r = out_ref.at[left, top]
    g_rr = remote(pass_r, pass_r, g_send.at[2], g_recv.at[2], to_r)
    g_rr.start()
    remote(from_r, from_r, g_send.at[1], g_recv.at[1], to_l).wait_recv()
    pass_l = out_ref.at[right, low]
    g_ll = remote(pass_l, pass_l, g_send.at[3], g_recv.at[3], to_l)
    g_ll.start()
    far_a, far_b = out_ref.at[far, top], out_ref.at[far, low]
    remote(far_a, far_a, g_send.at[2], g_recv.at[2], to_r).wait_recv()
    remote(far_b, far_b, g_send.at[3], g_recv.at[3], to_l).wait_recv()
    for copy in sends + [swap, on_r, on_l, g_r, g_l, g_rr, g_ll]:
        copy.wait_send()


VM = pl.BlockSpec(memory_space=pltpu.VMEM)
DMA = pltpu.SemaphoreType.DMA


def call(kernel, name, number, shapes, specs, scratch, args):
    return pl.pallas_call(
        kernel,
        name=name,
        out_shape=shapes,
        in_specs=specs,
        out_specs=jax.tree.map(lambda _: VM, shapes),
        scratch_shapes=scratch,
        compiler_params=pltpu.CompilerParams(
            collective_id=number, has_side_effects=True, vmem_limit_bytes=60 * 1024 * 1024
        ),
    )(*args)


def per_device(
    tokens_in, norm_gain, rec_query_weight, rec_forget_weight, rec_input_weight, att_query_weight,
    att_key_weight, att_value_weight, recurrence_output_weight, out_att_weight, floor_gap,
    decay_shift, rec_gain, att_gain, lambda_head,
):
    z, y, c, x = where_am_i()
    weights = jnp.stack(
        [
            w.reshape(16, 2, HEAD)
            for w in (
                rec_query_weight, rec_forget_weight, rec_input_weight,
                att_value_weight, att_query_weight, att_key_weight,
            )
        ],
        axis=2,
    )
    weights = weights.transpose(1, 0, 2, 3).reshape(2, 16, 6 * HEAD)
    linked = jnp.logical_and(z != 0, z != NZ - 1)
    start = (2 * y + c) * TOK + jnp.arange(TOK, dtype=jnp.int32)
    positions = jnp.stack([start, start + jnp.where(linked, 2 * NY * TOK, 0)]).astype(F32)
    width = PAIR // 2
    frequency = 1.0 / ROTARY_BASE ** (jnp.arange(width, dtype=F32) / width)
    angles = positions[:, :, None] * frequency
    cosine, sine = jnp.cos(angles), jnp.sin(angles)
    cosine = jnp.concatenate([cosine] * 4, axis=-1)
    sine = jnp.concatenate([-sine, sine] * 2, axis=-1)
    d_model = tokens_in.shape[1]
    rec, query, kv, shifts = call(
        project_kernel,
        "project",
        0,
        [
            jax.ShapeDtypeStruct((3, 2, TOK, HEAD), BF16),
            jax.ShapeDtypeStruct((2, TOK, HEAD), BF16),
            jax.ShapeDtypeStruct((2, TOK, 2 * HEAD), BF16),
            jax.ShapeDtypeStruct((2, TOK), F32),
        ],
        [VM] * 6,
        [
            pltpu.VMEM((NX, QUART, d_model), BF16),
            pltpu.VMEM((2, TOK, d_model), BF16),
            pltpu.VMEM((NZ, NY, 2, 16, 6 * HEAD), BF16),
            pltpu.VMEM((2, TOK), F32),
            DMA((1,)), DMA((1,)), DMA((4,)), DMA((4,)), DMA((1,)), DMA((1,)), DMA((NZ - 1,)), DMA((NZ - 1,)),
            *ring_sems(),
        ],
        (tokens_in.reshape(NX, QUART, d_model), weights, decay_shift, norm_gain[None], cosine, sine),
    )
    mix = call(
        mix_kernel,
        "mix",
        1,
        jax.ShapeDtypeStruct((2, TOK, 2 * HEAD), BF16),
        [VM] * 5 + [pl.BlockSpec(memory_space=pltpu.SMEM)] + [VM] * 2,
        [
            pltpu.VMEM((NY, 2, 2, TOK, 2 * HEAD), BF16),
            pltpu.VMEM((NY, 2, 2, ST_ROWS, HEAD), BF16),
            pltpu.VMEM((2, 2 * TOK, HEAD), BF16),
            pltpu.VMEM((2, 2 * TOK, HEAD), F32),
            pltpu.VMEM((2, 2 * TOK, HEAD), F32),
            pltpu.VMEM((2, 2 * TOK, HEAD), F32),
            pltpu.VMEM((2, TOK, HEAD), F32),
            pltpu.VMEM((2, TOK, HEAD), BF16),
            *ring_sems(),
            *ring_sems(),
        ],
        (
            rec, query, kv, shifts, floor_gap.reshape(2, HEAD), lambda_head, rec_gain[None], att_gain[None],
        ),
    )
    out = call(
        output_kernel,
        "output",
        2,
        jax.ShapeDtypeStruct((NX, QUART, d_model), BF16),
        [VM] * 3,
        [
            pltpu.VMEM((TOK, 2 * HEAD), BF16),
            pltpu.VMEM((NX, QUART, d_model), BF16),
            pltpu.VMEM((2, QUART // 2, d_model), BF16),
            pltpu.VMEM((3, QUART, d_model), BF16),
            DMA((1,)), DMA((1,)), DMA((6,)), DMA((6,)), DMA((4,)), DMA((4,)),
        ],
        (mix, recurrence_output_weight, out_att_weight),
    )
    return out.reshape(TOK, d_model)


def solution(mesh):
    split = Mesh(mesh.devices.reshape(NZ, NY, 2, NX), ("sp_0", "sp_1", "sp_2", "tp"))
    placed = (
        P(SP, None), P(), P(SP, "tp"), P(SP, "tp"), P(SP, "tp"), P(SP, "tp"), P(SP, "tp"), P(SP, "tp"),
        P("tp", None), P("tp", None), P("tp"), P("tp", SP), P(), P(), P("tp"),
    )
    return jax.shard_map(
        per_device, mesh=split, in_specs=placed, out_specs=P(SP, None), check_vma=False
    )
```

time: 638 us -> 136 us (0.21)
  the two profiles are of different devices: /device:TPU:184 before, /device:TPU:120 now
where the time goes in v1:
time: 136 us; the launch traced here: 135 us
  Pallas kernels  125 us (92%)
  local copies, waits for them, and re-layouts  7.35 us (5%)
  other arithmetic  2.98 us (2%)
    pallas_call x3, Pallas kernels, call(): pl.pallas_call(kernel, name=name, out_shape=shapes, in_specs=specs, out_s...  125 us
    unnamed x13, local copies, waits for them, and re-layouts  6.35 us

profile of v1, /device:TPU:120, one launch (start us, length us, event | category | flops | bytes accessed | tf_op | source)
XLA Modules:
  0.0 135.4 jit_solution(10605163972880477934)
XLA Ops:
  0.0 0.0 copy-start
  0.0 0.7 copy-done
  0.7 0.0 copy-start.1
  0.7 0.7 copy-done.1
  1.4 0.0 copy-start.2
  1.4 0.7 copy-done.2
  2.1 0.0 copy-start.3
  2.1 0.7 copy-done.3
  2.8 0.0 copy-start.4
  2.9 0.7 copy-done.4
  3.5 0.0 copy-start.5
  3.6 0.7 copy-done.5
  4.3 0.2 stack.8
  4.4 0.7 reshape.43.w_ref
  5.1 1.0 fusion
  6.1 1.0 pad_maximum_fusion.1.sin_ref
  7.1 1.0 pad_maximum_fusion.cos_ref
  8.1 44.9 %project.1 = (bf16[3,2,256,128]{3,2,1,0:T(8,128)(2,1)}, bf16[2,256,128]{2,1,0:T(8,128)(2,1)}, bf16[2,256,256]{2,1,0:T(8,128)(2,1)}, f32[2,256]{1,0:T(2,128)}) custom-call(bf16[4,64,2048]{2,1,0:T(8,128)(2,1)} %bitcast.8, bf16[2,16,768]{2,1,0:T(8,128)(2,1)} %reshape.43.w_ref, f32[2,256]{1,0:T(2,128)} %ds_ref.1, f32[1,2048]{1,0:T(1,128)} %bitcast.10, ...), custom_call_target="tpu_custom_call" | custom-call | tf_op jit(solution)/shard_map/project/pallas_call | solution.py:505
  53.0 45.0 %mix.1.mix_ref = bf16[2,256,256]{2,1,0:T(8,128)(2,1)} custom-call(bf16[3,2,256,128]{3,2,1,0:T(8,128)(2,1)} %get-tuple-element.9.rec_ref, bf16[2,256,128]{2,1,0:T(8,128)(2,1)} %get-tuple-element.10.q_ref, bf16[2,256,256]{2,1,0:T(8,128)(2,1)} %get-tuple-element.11.kv_ref, f32[2,256]{1,0:T(2,128)} %get-tuple-element.12.ds_ref, f32[2,128]{1,0:T(2,128)} %bitcast.11, ...), custom_call_target="tpu_custom_call" | custom-call | tf_op jit(solution)/shard_map/mix/pallas_call | solution.py:505
  98.0 35.1 %output.1 = bf16[4,64,2048]{2,1,0:T(8,128)(2,1)} custom-call(bf16[2,256,256]{2,1,0:T(8,128)(2,1)} %mix.1.mix_ref, bf16[256,2048]{1,0:T(8,128)(2,1)} %wr_ref.1, bf16[256,2048]{1,0:T(8,128)(2,1)} %wa_ref.1), custom_call_target="tpu_custom_call" | custom-call | tf_op jit(solution)/shard_map/output/pallas_call | solution.py:505
  133.1 2.3 %copy.29 = bf16[256,2048]{1,0:T(8,128)(2,1)} copy(bf16[256,2048]{1,0:T(8,128)(2,1)} %bitcast.7) | data formatting | bytes 2097152
  (15 shorter events, 0.2 us)
Async XLA Ops:
  0.0 0.7 copy-start
  0.7 0.7 copy-start.1
  1.4 0.7 copy-start.2
  2.1 0.7 copy-start.3
  2.8 0.7 copy-start.4
  3.5 0.7 copy-start.5

commit v2 on v1

v2 whole, which is shorter than its diff:
```python
import functools

import jax
import jax.numpy as jnp
import numpy as np
from jax import lax
from jax.experimental import pallas as pl
from jax.experimental.pallas import tpu as pltpu
from jax.sharding import Mesh
from jax.sharding import PartitionSpec as P

HEAD = 128
PAIR = 64
BLOCK = 64
SP = ("sp_0", "sp_1", "sp_2")
NZ, NY, NX = 8, 8, 4
HALF = NY // 2
TOK = 256
QUART = TOK // NX
ST_ROWS = 144
RECUR_EPSILON = 1e-06
ATTEND_EPSILON = 1e-05
ROTARY_BASE = 10000.0
SCORE_LOG2 = PAIR ** (-0.5) * 1.4426950408889634
F32, BF16 = jnp.float32, jnp.bfloat16
DMA = pltpu.SemaphoreType.DMA
VM = pl.BlockSpec(memory_space=pltpu.VMEM)
HBM = pl.BlockSpec(memory_space=pltpu.HBM)
OUT_HALF = 1024
VMEM_LIMIT = 60 * 1024 * 1024
REL = (0, 1, 7, 2, 6, 3, 5, 4)
POS = tuple(REL.index(d) for d in range(NZ))
MESH_ID = pl.DeviceIdType.MESH
NT = (((1,), (1,)), ((), ()))


def remote(src, dst, send, recv, where):
    return pltpu.make_async_remote_copy(
        src_ref=src, dst_ref=dst, send_sem=send, recv_sem=recv, device_id=where, device_id_type=MESH_ID
    )


def greet(places):
    barrier = pltpu.get_barrier_semaphore()
    for place in places:
        pl.semaphore_signal(barrier, inc=1, device_id=place, device_id_type=MESH_ID)
    pl.semaphore_wait(barrier, len(places))


def where_am_i():
    return (lax.axis_index("sp_0"), lax.axis_index("sp_1"), lax.axis_index("sp_2"), lax.axis_index("tp"))


def partner_row(z):
    return jnp.where(z % 2 == 1, (z + 1) % NZ, (z + NZ - 1) % NZ)


class Ring:
    def __init__(self, y, c, parts, piece, sems):
        self.y, self.c, self.parts, self.piece = y, c, parts, piece
        self.sr, self.rr, self.sl, self.rl, self.sp, self.rp = sems
        self.right = {"sp_1": (y + 1) % NY}
        self.left = {"sp_1": (y + NY - 1) % NY}
        self.other = {"sp_2": 1 - c}

    def at(self, offset, i):
        return self.piece((self.y + offset + NY) % NY, self.c, i)

    def index(self, k, i):
        return self.parts * (k - 1) + i

    def to_right(self, k, i):
        ref, n = self.at(1 - k, i), self.index(k, i)
        return remote(ref, ref, self.sr.at[n], self.rr.at[n], self.right)

    def to_left(self, k, i):
        ref, n = self.at(k - 1, i), self.index(k, i)
        return remote(ref, ref, self.sl.at[n], self.rl.at[n], self.left)

    def to_other(self, offset, i):
        ref, n = self.at(offset, i), self.parts * (offset % NY) + i
        return remote(ref, ref, self.sp.at[n], self.rp.at[n], self.other)

    def goes_right(self, k, i):
        return k < HALF or (k == HALF and i < self.parts // 2)

    def goes_left(self, k, i):
        return k < HALF or (k == HALF and i >= self.parts // 2)

    def begin(self, i):
        self.to_right(1, i).start()
        self.to_left(1, i).start()
        self.to_other(0, i).start()

    def step(self, k, i):
        n = self.index(k, i)
        if self.goes_right(k, i):
            ref = self.at(-k, i)
            remote(ref, ref, self.sr.at[n], self.rr.at[n], self.right).wait_recv()
            if self.goes_right(k + 1, i):
                self.to_right(k + 1, i).start()
            self.to_other(-k, i).start()
        if self.goes_left(k, i):
            ref = self.at(k, i)
            remote(ref, ref, self.sl.at[n], self.rl.at[n], self.left).wait_recv()
            if self.goes_left(k + 1, i):
                self.to_left(k + 1, i).start()
            self.to_other(k, i).start()

    def wait_other(self, offset):
        for i in range(self.parts):
            ref = self.piece((self.y + offset + NY) % NY, 1 - self.c, i)
            n = self.parts * (offset % NY) + i
            remote(ref, ref, self.sp.at[n], self.rp.at[n], self.other).wait_recv()

    def finish(self):
        for i in range(self.parts):
            for k in range(1, HALF + 1):
                if self.goes_right(k, i):
                    self.to_right(k, i).wait_send()
                if self.goes_left(k, i):
                    self.to_left(k, i).wait_send()
            for offset in range(NY):
                self.to_other(offset, i).wait_send()


def ring_sems(parts):
    return [DMA((parts * HALF,))] * 4 + [DMA((parts * NY,))] * 2


def layer_kernel(
    x_ref, wq_ref, wf_ref, wi_ref, wv_ref, waq_ref, wak_ref, wr_ref, wa_ref,
    ds_hbm, gain_hbm, freq_hbm, fg_hbm, rgain_hbm, again_hbm, lam_ref,
    out_ref,
    ds_ref, gain_ref, freq_ref, fg_ref, rgain_ref, again_ref,
    xloc, xp, xn, wloc, wbuf, dsp, dso, wobuf,
    rec, kvbuf, stbuf, q2, m_s, l_s, acc, local, qdec, mixs, mb,
    load, t1s, t1r, t2s, t2r, dss, dsr, w1s, w1r, wos, wor, wops, wopr, as_, ar, gs, gr,
    *sems,
):
    z, y, c, x = where_am_i()
    zp = partner_row(z)
    row = (z + 1) % 2
    linked = jnp.logical_and(z != 0, z != NZ - 1)
    right, left, far = (x + 1) % NX, (x + NX - 1) % NX, (x + 2) % NX
    to_r, to_l, core = {"tp": right}, {"tp": left}, {"sp_2": 1 - c}
    half = QUART // 2
    halves = (pl.ds(0, half), pl.ds(half, half))

    loads = []

    def bring(src, dst):
        copy = pltpu.make_async_copy(src, dst, load.at[len(loads)])
        copy.start()
        loads.append(copy)
        return copy

    mine = pl.ds(pl.multiple_of(row * HEAD, HEAD), HEAD)
    yours = pl.ds(pl.multiple_of((1 - row) * HEAD, HEAD), HEAD)
    weight_refs = (wq_ref, wf_ref, wi_ref, wv_ref, waq_ref, wak_ref)
    own_w = [
        bring(ref.at[:, mine], wbuf.at[0, y, c, :, pl.ds(p * HEAD, HEAD)])
        for p, ref in enumerate(weight_refs)
    ]
    other_w = [
        bring(ref.at[:, yours], wloc.at[:, pl.ds(p * HEAD, HEAD)]) for p, ref in enumerate(weight_refs)
    ]
    quarter = bring(x_ref.at[x], xloc.at[x])
    rest_x = [bring(x_ref.at[(x + d) % NX], xloc.at[(x + d) % NX]) for d in range(1, NX)]
    own_wo = [
        bring(ref.at[:, pl.ds(h * OUT_HALF, OUT_HALF)], wobuf.at[x, h, pl.ds(r * 2 * HEAD, 2 * HEAD)])
        for h in range(2)
        for r, ref in enumerate((wr_ref, wa_ref))
    ]

    small = [
        bring(src, dst)
        for src, dst in (
            (ds_hbm, ds_ref), (gain_hbm, gain_ref), (freq_hbm, freq_ref), (fg_hbm, fg_ref),
            (rgain_hbm, rgain_ref), (again_hbm, again_ref),
        )
    ]
    greet(
        [{"sp_0": (z + d) % NZ} for d in range(1, NZ)]
        + [{"tp": (x + d) % NX} for d in range(1, NX)]
        + [{"sp_0": zp, "tp": (x + d) % NX} for d in range(1, NX)]
        + [{"sp_1": (y + 1) % NY}, {"sp_1": (y + NY - 1) % NY}, core]
    )

    def to_row(d):
        src = wbuf.at[0, y, c] if d % 2 == 0 else wloc
        at = POS[(NZ - d) % NZ]
        return remote(
            src, wbuf.at[at, y, c], w1s.at[at - 1], w1r.at[at - 1], {"sp_0": (z + d) % NZ}
        )

    def row_came(at):
        ref = wbuf.at[at, y, c]
        remote(ref, ref, w1s.at[at - 1], w1r.at[at - 1], core).wait_recv()

    spread = {d: to_row(d) for d in range(1, NZ)}
    across = [
        remote(xloc.at[x, rows], xp.at[x, rows], t1s.at[i], t1r.at[i], {"sp_0": zp})
        for i, rows in enumerate(halves)
    ]
    shifts = remote(ds_ref, dsp, dss.at[0], dsr.at[0], {"sp_0": zp})
    for copy in other_w:
        copy.wait()
    spread[1].start()
    spread[7].start()
    quarter.wait()
    across[0].start()
    across[1].start()
    for copy in own_w:
        copy.wait()
    for d in (2, 6, 3, 5, 4):
        spread[d].start()
    for copy in small:
        copy.wait()
    shifts.start()

    for copy in own_wo:
        copy.wait()

    def wo_at(group, i):
        return wobuf.at[group, c, pl.ds(i * HEAD, HEAD)]

    wo_right = [remote(wo_at(x, i), wo_at(x, i), wos.at[i], wor.at[i], to_r) for i in range(4)]
    wo_left = [remote(wo_at(x, i), wo_at(x, i), wos.at[4 + i], wor.at[4 + i], to_l) for i in range(4)]
    wo_on_right = [
        remote(wo_at(left, i), wo_at(left, i), wos.at[8 + i], wor.at[8 + i], to_r) for i in (0, 1)
    ]
    wo_on_left = [
        remote(wo_at(right, i), wo_at(right, i), wos.at[8 + i], wor.at[8 + i], to_l) for i in (2, 3)
    ]
    wo_push = {
        (g, i): remote(
            wo_at((x + g) % NX, i),
            wo_at((x + g) % NX, i),
            wops.at[4 * (g - 1) + i],
            wopr.at[4 * (g - 1) + i],
            core,
        )
        for g in (1, 2, 3)
        for i in range(4)
    }

    def wo_came(group_offset, i, slot):
        ref = wo_at((x + group_offset) % NX, i)
        remote(ref, ref, wos.at[slot], wor.at[slot], to_r).wait_recv()
        wo_push[(group_offset, i)].start()

    wo_right[0].start()
    wo_left[2].start()

    w_ring = Ring(
        y, c, 4, lambda yo, stream, i: wbuf.at[pl.ds(2 * i, 2), yo, stream], sems[0:6]
    )

    def normed(source, kind, i):
        values = source[i].astype(F32)
        mean_sq = jnp.mean(values * values, axis=-1, keepdims=True)
        scale = lax.rsqrt(mean_sq + RECUR_EPSILON)
        for p in range(NZ):
            cols = pl.ds(pl.multiple_of(((z + REL[p]) % NZ) * 256, 256), 256)
            value = source[i, :, cols].astype(F32) * scale * gain_ref[:, cols]
            xn[kind, pl.ds(pl.multiple_of(i * QUART, QUART), QUART), pl.ds(p * 256, 256)] = value.astype(BF16)

    t2_right = [remote(xp.at[x, r], xp.at[x, r], t2s.at[i], t2r.at[i], to_r) for i, r in enumerate(halves)]
    t2_left = [remote(xp.at[x, r], xp.at[x, r], t2s.at[2 + i], t2r.at[2 + i], to_l) for i, r in enumerate(halves)]
    t2_on_right = remote(xp.at[left, halves[0]], xp.at[left, halves[0]], t2s.at[4], t2r.at[4], to_r)
    t2_on_left = remote(xp.at[right, halves[1]], xp.at[right, halves[1]], t2s.at[5], t2r.at[5], to_l)

    def t2_came(group, i, slot):
        ref = xp.at[group, halves[i]]
        remote(ref, ref, t2s.at[slot], t2r.at[slot], to_r).wait_recv()

    row_came(1)
    w_ring.begin(0)
    row_came(2)
    row_came(3)
    w_ring.begin(1)
    for i in range(2):
        across[i].wait_recv()
        t2_right[i].start()
        t2_left[i].start()
        row_came(4 + 2 * i)
        row_came(5 + 2 * i)
        w_ring.begin(2 + i)
    for copy in rest_x:
        copy.wait()
    for i in range(NX):
        w_ring.step(1, i)
        normed(xloc, row, i)
    t2_came(left, 0, 0)
    t2_on_right.start()
    t2_came(right, 1, 3)
    t2_on_left.start()
    for i in (1, 2, 3):
        wo_right[i].start()
    for i in (3, 0, 1):
        wo_left[i].start()
    normed(xp, 1 - row, x)
    t2_came(left, 1, 1)
    t2_came(right, 0, 2)
    for i in range(4):
        w_ring.step(2, i)
        if i == 1:
            normed(xp, 1 - row, left)
        elif i == 3:
            normed(xp, 1 - row, right)
    for i in range(4):
        w_ring.step(3, i)
    t2_came(far, 0, 4)
    t2_came(far, 1, 5)
    normed(xp, 1 - row, far)
    wo_came(3, 0, 0)
    wo_on_right[0].start()
    wo_came(1, 2, 6)
    wo_on_left[0].start()

    lane = lax.broadcasted_iota(jnp.int32, (TOK, HEAD), 1)
    first = (lane % PAIR) < (PAIR // 2)
    place = (2 * y + c) * TOK + lax.broadcasted_iota(jnp.int32, (TOK, HEAD), 0)
    tables = []
    for kind in range(2):
        at = place if kind == 0 else place + jnp.where(linked, 2 * NY * TOK, 0)
        angle = at.astype(F32) * freq_ref[...]
        sine = jnp.sin(angle)
        tables.append((jnp.cos(angle), jnp.where(first, -sine, sine)))
        m_s[kind, pl.ds(0, TOK)] = tables[kind][0]
        l_s[kind, pl.ds(0, TOK)] = tables[kind][1]

    def turned(values, kind):
        swapped = jnp.where(
            first, pltpu.roll(values, HEAD - PAIR // 2, 1), pltpu.roll(values, PAIR // 2, 1)
        )
        return values * m_s[kind, pl.ds(0, TOK)] + swapped * l_s[kind, pl.ds(0, TOK)]

    shifts.wait_recv()
    dso[pl.ds(row, 1)] = ds_ref[pl.ds(row, 1)]
    dso[pl.ds(1 - row, 1)] = dsp[pl.ds(row, 1)]
    for i in range(4):
        w_ring.step(4, i)
    for offset in range(NY):
        w_ring.wait_other(offset)

    def projected(part, kind):
        weight = wbuf[:, :, :, :, pl.ds(part * 256, 256)].reshape(NZ * NY * 2 * 16, 256)
        out = jnp.dot(xn[kind], weight, preferred_element_type=F32)
        return out[:, :HEAD], out[:, HEAD:]

    half_rows = TOK // 2
    kv_ring = Ring(
        y,
        c,
        4,
        lambda yo, stream, i: kvbuf.at[yo, i // 2, stream, pl.ds((i % 2) * half_rows, half_rows)],
        sems[6:12],
    )
    st_ring = Ring(y, c, 2, lambda yo, stream, i: stbuf.at[yo, stream, i], sems[12:18])
    for kind in range(2):
        one, two = projected(2, kind)
        kvbuf[y, kind, c, :, pl.ds(0, HEAD)] = turned(two, kind).astype(BF16)
        query = turned(one, kind)
        q2[kind, pl.ds(0, TOK)] = jnp.where(lane < PAIR, query, 0.0).astype(BF16)
        q2[kind, pl.ds(TOK, TOK)] = jnp.where(lane >= PAIR, query, 0.0).astype(BF16)
        one, two = projected(1, kind)
        kvbuf[y, kind, c, :, pl.ds(HEAD, HEAD)] = two.astype(BF16)
        rec[2, kind] = one.astype(BF16)
    kv_ring.begin(0)
    kv_ring.begin(1)
    for kind in range(2):
        one, two = projected(0, kind)
        rec[0, kind] = one.astype(BF16)
        rec[1, kind] = two.astype(BF16)
        if kind == 0:
            kv_ring.begin(2)
            kv_ring.begin(3)

    causal = lax.broadcasted_iota(jnp.int32, (BLOCK, BLOCK), 0) >= lax.broadcasted_iota(
        jnp.int32, (BLOCK, BLOCK), 1
    )
    tril = jnp.where(causal, 1.0, 0.0).astype(F32)
    gap = fg_ref[pl.ds(row, 1)]

    def segment(kind):
        shift = jnp.broadcast_to(dso[pl.ds(kind, 1)], (HEAD, TOK)).T
        state = jnp.zeros((HEAD, HEAD), F32)
        total = jnp.zeros((1, HEAD), F32)
        for b in range(TOK // BLOCK):
            rows = pl.ds(b * BLOCK, BLOCK)
            forget = rec[1, kind, rows].astype(F32)
            query = rec[0, kind, rows].astype(F32)
            value = rec[2, kind, rows]
            gate = gap * (1.0 / (1.0 + jnp.exp(forget)))
            decay = jnp.log1p(-gate) + shift[b * BLOCK : (b + 1) * BLOCK]
            cum = jnp.dot(tril, decay, precision=lax.Precision.HIGHEST, preferred_element_type=F32)
            end = cum[BLOCK - 1 :, :]
            q_dec = query * jnp.exp(cum)
            qdec[kind, rows] = (q_dec * jnp.exp(total)).astype(BF16)
            q_dec = q_dec.astype(BF16)
            k_grow = (gate * jnp.exp(-cum)).astype(BF16)
            scores = lax.dot_general(q_dec, k_grow, NT, preferred_element_type=F32)
            scores = jnp.where(causal, scores, 0.0).astype(BF16)
            out = jnp.dot(scores, value, preferred_element_type=F32)
            if b > 0:
                out = out + lax.dot_general(q_dec, state.astype(BF16), NT, preferred_element_type=F32)
            local[kind, rows] = out
            k_end = (gate * jnp.exp(end - cum)).astype(BF16)
            fresh = jnp.dot(value.astype(F32).T.astype(BF16), k_end, preferred_element_type=F32)
            state = state * jnp.exp(end) + fresh
            total = total + end
        stbuf[y, c, kind, pl.ds(0, HEAD)] = state.astype(BF16)
        high = total.astype(BF16)
        rest = total - high.astype(F32)
        middle = rest.astype(BF16)
        low = (rest - middle.astype(F32)).astype(BF16)
        index = lax.broadcasted_iota(jnp.int32, (ST_ROWS - HEAD, HEAD), 0)
        stack = jnp.where(
            index == 0, high.astype(F32), jnp.where(index == 1, middle.astype(F32), low.astype(F32))
        )
        stbuf[y, c, kind, pl.ds(HEAD, ST_ROWS - HEAD)] = stack.astype(BF16)

    segment(0)
    kv_ring.step(1, 0)
    kv_ring.step(1, 1)
    segment(1)
    kv_ring.step(1, 2)
    kv_ring.step(1, 3)
    st_ring.begin(0)
    st_ring.begin(1)

    def keys_values(yo, kind):
        both = kvbuf[yo, kind].reshape(2 * TOK, 2 * HEAD)
        return both[:, :HEAD], both[:, HEAD:]

    kv_ring.wait_other(0)

    def own(kind, carry):
        keys, values = keys_values(y, kind)
        for part in range(2):
            rows = pl.ds(part * TOK, TOK)
            scores = lax.dot_general(q2[kind, rows], keys, NT, preferred_element_type=F32)
            seen = lax.broadcasted_iota(jnp.int32, (TOK, 2 * TOK), 1) <= (
                lax.broadcasted_iota(jnp.int32, (TOK, 2 * TOK), 0) + c * TOK
            )
            scores = jnp.where(seen, scores, -jnp.inf)
            best = jnp.max(scores, axis=-1, keepdims=True)
            expo = jnp.exp2((scores - best) * SCORE_LOG2)
            m_s[kind, rows] = jnp.broadcast_to(best, (TOK, HEAD))
            l_s[kind, rows] = jnp.broadcast_to(jnp.sum(expo, axis=-1, keepdims=True), (TOK, HEAD))
            acc[kind, rows] = jnp.dot(expo.astype(BF16), values, preferred_element_type=F32)
        return carry

    lax.fori_loop(0, 2, own, 0)

    def absorb(yo, q_kind, kv_kind):
        keys, values = keys_values(yo, kv_kind)
        for part in range(2):
            rows = pl.ds(part * TOK, TOK)
            scores = lax.dot_general(q2[q_kind, rows], keys, NT, preferred_element_type=F32)
            old = m_s[q_kind, rows]
            best = jnp.maximum(old, jnp.max(scores, axis=-1, keepdims=True))
            scale = jnp.exp2((old - best) * SCORE_LOG2)
            expo = jnp.exp2((scores - best[:, :1]) * SCORE_LOG2)
            m_s[q_kind, rows] = best
            l_s[q_kind, rows] = l_s[q_kind, rows] * scale + jnp.sum(expo, axis=-1, keepdims=True)
            acc[q_kind, rows] = acc[q_kind, rows] * scale + jnp.dot(
                expo.astype(BF16), values, preferred_element_type=F32
            )

    def process(offset):
        if offset:
            kv_ring.wait_other(offset)
        yo = (y + offset + NY) % NY

        def unit(kind_at, carry):
            q_kind = jnp.where(kind_at == 0, 0, 1)
            kv_kind = jnp.where(kind_at == 2, 1, 0)
            wanted = jnp.where(kind_at == 1, linked.astype(jnp.int32), (yo < y).astype(jnp.int32))

            @pl.when(wanted == 1)
            def _():
                absorb(yo, q_kind, kv_kind)

            return carry

        lax.fori_loop(0, 3, unit, 0)

    process(0)
    for k in range(2, HALF + 1):
        kv_ring.step(k, 0)
        kv_ring.step(k, 1)
        process(1 - k)
        kv_ring.step(k, 2)
        kv_ring.step(k, 3)
        st_ring.step(k - 1, 0)
        st_ring.step(k - 1, 1)
        if k == 3:
            wo_came(3, 1, 1)
            wo_on_right[1].start()
            wo_came(1, 3, 7)
            wo_on_left[1].start()
        process(k - 1)
    st_ring.step(HALF, 0)
    st_ring.step(HALF, 1)
    process(HALF)
    for offset in range(NY):
        st_ring.wait_other(offset)

    me = 2 * y + c

    def pass_on(kind, s, state):
        yo, stream = s // 2, s % 2
        tail = stbuf[yo, stream, kind, pl.ds(HEAD, ST_ROWS - HEAD)].astype(F32)
        total = tail[0:1] + tail[1:2] + tail[2:3]
        return state * jnp.exp(total) + stbuf[yo, stream, kind, pl.ds(0, HEAD)].astype(F32)

    nothing = jnp.zeros((HEAD, HEAD), F32)
    into_low = lax.fori_loop(0, me, functools.partial(pass_on, 0), nothing)
    all_low = lax.fori_loop(me, 2 * NY, functools.partial(pass_on, 0), into_low)
    all_low = all_low * jnp.where(linked, 1.0, 0.0)
    into_high = lax.fori_loop(0, me, functools.partial(pass_on, 1), all_low)
    lam = lam_ref[row]

    def mix_to(same, d):
        kind = row if same else 1 - row
        there = (x + d) % NX
        n = d if same else NX + d
        where = {"tp": there} if same else {"sp_0": zp, "tp": there}
        return remote(mixs.at[kind, there], mb.at[x, row], as_.at[n], ar.at[n], where)

    for kind in range(2):
        state = (into_low if kind == 0 else into_high).astype(BF16)
        raw = local[kind] + lax.dot_general(qdec[kind], state, NT, preferred_element_type=F32)
        mean_sq = jnp.mean(raw * raw, axis=-1, keepdims=True)
        rec_mix = (raw * lax.rsqrt(mean_sq + RECUR_EPSILON) * rgain_ref[...]).astype(BF16)
        raw = acc[kind, pl.ds(0, TOK)] / l_s[kind, pl.ds(0, TOK)] - lam * (
            acc[kind, pl.ds(TOK, TOK)] / l_s[kind, pl.ds(TOK, TOK)]
        )
        mean_sq = jnp.mean(raw * raw, axis=-1, keepdims=True)
        att_mix = (raw * lax.rsqrt(mean_sq + ATTEND_EPSILON) * again_ref[...]).astype(BF16)
        for i in range(NX):
            mixs[kind, i, :, pl.ds(0, HEAD)] = rec_mix[i * QUART : (i + 1) * QUART]
            mixs[kind, i, :, pl.ds(HEAD, HEAD)] = att_mix[i * QUART : (i + 1) * QUART]

    mix_sends = [mix_to(False, d) for d in (2, 1, 3, 0)] + [mix_to(True, d) for d in (2, 1, 3)]
    for copy in mix_sends:
        copy.start()
    mb[x, row] = mixs[row, x]

    for i in (1, 2, 3):
        if i != 1:
            wo_came(3, i, i)
    for i in (0, 1):
        wo_came(1, i, 4 + i)
    for i in range(4):
        wo_came(2, i, 8 + i)
    for g in (1, 2, 3):
        for i in range(4):
            ref = wobuf.at[(x + g) % NX, 1 - c, pl.ds(i * HEAD, HEAD)]
            remote(ref, ref, wops.at[4 * (g - 1) + i], wopr.at[4 * (g - 1) + i], core).wait_recv()

    for d in range(NX):
        for same in (True, False):
            if same and d == 0:
                continue
            n = d if same else NX + d
            ref = mb.at[(x + NX - d) % NX, row if same else 1 - row]
            remote(ref, ref, as_.at[n], ar.at[n], core).wait_recv()

    width = OUT_HALF // 2
    groups = [
        jnp.concatenate([mb[g, h][:, p * HEAD : (p + 1) * HEAD] for p in range(2) for h in range(2)], axis=1)
        for g in range(NX)
    ]
    gathers = []
    for j in range(4):
        total = jnp.zeros((QUART, width), F32)
        for g in range(NX):
            weight = wobuf[g, j // 2, :, pl.ds((j % 2) * width, width)]
            total += jnp.dot(groups[g], weight, preferred_element_type=F32).astype(BF16).astype(F32)
        cols = pl.ds(j * width, width)
        out_ref[x, :, cols] = total.astype(BF16)
        ref = out_ref.at[x, :, cols]
        gathers.append(remote(ref, ref, gs.at[4 * j], gr.at[4 * j], to_r))
        gathers.append(remote(ref, ref, gs.at[4 * j + 1], gr.at[4 * j + 1], to_l))
        gathers[-2].start()
        gathers[-1].start()
    for j in range(4):
        cols = pl.ds(j * width, width)
        ref = out_ref.at[left, :, cols]
        remote(ref, ref, gs.at[4 * j], gr.at[4 * j], to_r).wait_recv()
        ref = out_ref.at[left, halves[0], cols]
        gathers.append(remote(ref, ref, gs.at[4 * j + 2], gr.at[4 * j + 2], to_r))
        gathers[-1].start()
        ref = out_ref.at[right, :, cols]
        remote(ref, ref, gs.at[4 * j + 1], gr.at[4 * j + 1], to_l).wait_recv()
        ref = out_ref.at[right, halves[1], cols]
        gathers.append(remote(ref, ref, gs.at[4 * j + 3], gr.at[4 * j + 3], to_l))
        gathers[-1].start()
    for j in range(4):
        cols = pl.ds(j * width, width)
        for i in range(2):
            ref = out_ref.at[far, halves[i], cols]
            remote(ref, ref, gs.at[4 * j + 2 + i], gr.at[4 * j + 2 + i], to_r).wait_recv()
    w_ring.finish()
    kv_ring.finish()
    st_ring.finish()
    sent = list(spread.values()) + across + [shifts] + t2_right + t2_left + [t2_on_right, t2_on_left]
    sent += wo_right + wo_left + wo_on_right + wo_on_left + list(wo_push.values()) + mix_sends + gathers
    for copy in sent:
        copy.wait_send()


def per_device(
    tokens_in, norm_gain, rec_query_weight, rec_forget_weight, rec_input_weight, att_query_weight,
    att_key_weight, att_value_weight, recurrence_output_weight, out_att_weight, floor_gap,
    decay_shift, rec_gain, att_gain, lambda_head,
):
    width = PAIR // 2
    steps = np.arange(width, dtype=np.float32) / np.float32(width)
    frequency = np.float32(1.0) / np.float32(ROTARY_BASE) ** steps
    frequency = np.concatenate([frequency] * 4)[None].astype(np.float32)
    d_model = tokens_in.shape[1]
    out = pl.pallas_call(
        layer_kernel,
        name="layer",
        out_shape=jax.ShapeDtypeStruct((NX, QUART, d_model), BF16),
        in_specs=[HBM] * 15 + [pl.BlockSpec(memory_space=pltpu.SMEM)],
        out_specs=VM,
        scratch_shapes=[
            pltpu.VMEM((2, TOK), F32),
            pltpu.VMEM((1, d_model), F32),
            pltpu.VMEM((1, HEAD), F32),
            pltpu.VMEM((2, HEAD), F32),
            pltpu.VMEM((1, HEAD), F32),
            pltpu.VMEM((1, HEAD), F32),
            pltpu.VMEM((NX, QUART, d_model), BF16),
            pltpu.VMEM((NX, QUART, d_model), BF16),
            pltpu.VMEM((2, TOK, d_model), BF16),
            pltpu.VMEM((16, 6 * HEAD), BF16),
            pltpu.VMEM((NZ, NY, 2, 16, 6 * HEAD), BF16),
            pltpu.VMEM((2, TOK), F32),
            pltpu.VMEM((2, TOK), F32),
            pltpu.VMEM((NX, 2, 4 * HEAD, OUT_HALF), BF16),
            pltpu.VMEM((3, 2, TOK, HEAD), BF16),
            pltpu.VMEM((NY, 2, 2, TOK, 2 * HEAD), BF16),
            pltpu.VMEM((NY, 2, 2, ST_ROWS, HEAD), BF16),
            pltpu.VMEM((2, 2 * TOK, HEAD), BF16),
            pltpu.VMEM((2, 2 * TOK, HEAD), F32),
            pltpu.VMEM((2, 2 * TOK, HEAD), F32),
            pltpu.VMEM((2, 2 * TOK, HEAD), F32),
            pltpu.VMEM((2, TOK, HEAD), F32),
            pltpu.VMEM((2, TOK, HEAD), BF16),
            pltpu.VMEM((2, NX, QUART, 2 * HEAD), BF16),
            pltpu.VMEM((NX, 2, QUART, 2 * HEAD), BF16),
            DMA((26,)),
            DMA((2,)), DMA((2,)), DMA((6,)), DMA((6,)), DMA((1,)), DMA((1,)),
            DMA((NZ - 1,)), DMA((NZ - 1,)), DMA((12,)), DMA((12,)), DMA((12,)), DMA((12,)),
            DMA((2 * NX,)), DMA((2 * NX,)), DMA((16,)), DMA((16,)),
            *ring_sems(4), *ring_sems(4), *ring_sems(2),
        ],
        compiler_params=pltpu.CompilerParams(
            collective_id=0, has_side_effects=True, vmem_limit_bytes=VMEM_LIMIT
        ),
    )(
        tokens_in.reshape(NX, QUART, d_model), rec_query_weight, rec_forget_weight, rec_input_weight,
        att_value_weight, att_query_weight, att_key_weight, recurrence_output_weight, out_att_weight,
        decay_shift, norm_gain[None], jnp.asarray(frequency), floor_gap.reshape(2, HEAD),
        rec_gain[None], att_gain[None], lambda_head,
    )
    return out.reshape(TOK, d_model)


def solution(mesh):
    split = Mesh(mesh.devices.reshape(NZ, NY, 2, NX), ("sp_0", "sp_1", "sp_2", "tp"))
    placed = (
        P(SP, None), P(), P(SP, "tp"), P(SP, "tp"), P(SP, "tp"), P(SP, "tp"), P(SP, "tp"), P(SP, "tp"),
        P("tp", None), P("tp", None), P("tp"), P("tp", SP), P(), P(), P("tp"),
    )
    return jax.shard_map(
        per_device, mesh=split, in_specs=placed, out_specs=P(SP, None), check_vma=False
    )
```

time: 136 us -> 103 us (0.76)
  the two profiles are of different devices: /device:TPU:120 before, /device:TPU:1 now
where the time goes in v2:
time: 103 us; the launch traced here: 102 us
  Pallas kernels  99.7 us (97%)
  local copies, waits for them, and re-layouts  2.3 us (2%)
    pallas_call x1, Pallas kernels, per_device(): pl.pallas_call(layer_kernel, name='layer', out_shape=jax.ShapeDtypeStruct...  99.7 us
    unnamed x1, local copies, waits for them, and re-layouts  2.3 us

profile of v2, /device:TPU:1, one launch (start us, length us, event | category | flops | bytes accessed | tf_op | source)
XLA Modules:
  0.0 102.0 jit_solution(14735828432713853465)
XLA Ops:
  0.0 99.7 %layer.1 = bf16[4,64,2048]{2,1,0:T(8,128)(2,1)} custom-call(bf16[4,64,2048]{2,1,0:T(8,128)(2,1)} %bitcast.7, bf16[16,256]{1,0:T(8,128)(2,1)} %wq_ref.1, bf16[16,256]{1,0:T(8,128)(2,1)} %wf_ref.1, bf16[16,256]{1,0:T(8,128)(2,1)} %wi_ref.1, bf16[16,256]{1,0:T(8,128)(2,1)} %wv_ref.1, bf16[16,256]{1,0:T(8,128)(2,1)} %waq_ref.1, bf16[16,256]{1,0:T(8,128)(2,1)} %wak_ref.1, ...), custom_call_target="tpu_custom_call" | custom-call | tf_op jit(solution)/shard_map/layer/pallas_call | solution.py:627
  99.7 2.3 %copy.18 = bf16[256,2048]{1,0:T(8,128)(2,1)} copy(bf16[256,2048]{1,0:T(8,128)(2,1)} %bitcast.6) | data formatting | bytes 2097152

commit v3 on v2

--- a/solution.py
+++ b/solution.py
@@ -17,7 +17,7 @@
 HALF = NY // 2
 TOK = 256
 QUART = TOK // NX
-ST_ROWS = 144
+ST_ROWS = 160
 RECUR_EPSILON = 1e-06
 ATTEND_EPSILON = 1e-05
 ROTARY_BASE = 10000.0
@@ -131,11 +131,11 @@
 def layer_kernel(
     x_ref, wq_ref, wf_ref, wi_ref, wv_ref, waq_ref, wak_ref, wr_ref, wa_ref,
     ds_hbm, gain_hbm, freq_hbm, fg_hbm, rgain_hbm, again_hbm, lam_ref,
-    out_ref,
-    ds_ref, gain_ref, freq_ref, fg_ref, rgain_ref, again_ref,
+    res_ref,
+    out_ref, ds_ref, gain_ref, freq_ref, fg_ref, rgain_ref, again_ref,
     xloc, xp, xn, wloc, wbuf, dsp, dso, wobuf,
-    rec, kvbuf, stbuf, q2, m_s, l_s, acc, local, qdec, mixs, mb,
-    load, t1s, t1r, t2s, t2r, dss, dsr, w1s, w1r, wos, wor, wops, wopr, as_, ar, gs, gr,
+    rec, kvbuf, stbuf, pair, q2, m_s, l_s, acc, local, qdec, give, gm, sums,
+    load, t1s, t1r, t2s, t2r, dss, dsr, w1s, w1r, wos, wor, wops, wopr, ms, mr, put, prs, prr,
     *sems,
 ):
     z, y, c, x = where_am_i()
@@ -146,6 +146,7 @@
     to_r, to_l, core = {"tp": right}, {"tp": left}, {"sp_2": 1 - c}
     half = QUART // 2
     halves = (pl.ds(0, half), pl.ds(half, half))
+    pieces = tuple(pl.ds(i * (QUART // 4), QUART // 4) for i in range(4))
 
     loads = []
 
@@ -182,8 +183,7 @@
     ]
     greet(
         [{"sp_0": (z + d) % NZ} for d in range(1, NZ)]
-        + [{"tp": (x + d) % NX} for d in range(1, NX)]
-        + [{"sp_0": zp, "tp": (x + d) % NX} for d in range(1, NX)]
+        + [to_r, to_l]
         + [{"sp_1": (y + 1) % NY}, {"sp_1": (y + NY - 1) % NY}, core]
     )
 
@@ -201,20 +201,20 @@
     spread = {d: to_row(d) for d in range(1, NZ)}
     across = [
         remote(xloc.at[x, rows], xp.at[x, rows], t1s.at[i], t1r.at[i], {"sp_0": zp})
-        for i, rows in enumerate(halves)
+        for i, rows in enumerate(pieces)
     ]
     shifts = remote(ds_ref, dsp, dss.at[0], dsr.at[0], {"sp_0": zp})
     for copy in other_w:
         copy.wait()
     spread[1].start()
     spread[7].start()
-    quarter.wait()
-    across[0].start()
-    across[1].start()
     for copy in own_w:
         copy.wait()
     for d in (2, 6, 3, 5, 4):
         spread[d].start()
+    quarter.wait()
+    for copy in across:
+        copy.start()
     for copy in small:
         copy.wait()
     shifts.start()
@@ -266,53 +266,64 @@
             value = source[i, :, cols].astype(F32) * scale * gain_ref[:, cols]
             xn[kind, pl.ds(pl.multiple_of(i * QUART, QUART), QUART), pl.ds(p * 256, 256)] = value.astype(BF16)
 
-    t2_right = [remote(xp.at[x, r], xp.at[x, r], t2s.at[i], t2r.at[i], to_r) for i, r in enumerate(halves)]
-    t2_left = [remote(xp.at[x, r], xp.at[x, r], t2s.at[2 + i], t2r.at[2 + i], to_l) for i, r in enumerate(halves)]
-    t2_on_right = remote(xp.at[left, halves[0]], xp.at[left, halves[0]], t2s.at[4], t2r.at[4], to_r)
-    t2_on_left = remote(xp.at[right, halves[1]], xp.at[right, halves[1]], t2s.at[5], t2r.at[5], to_l)
+    t2_right = [remote(xp.at[x, r], xp.at[x, r], t2s.at[i], t2r.at[i], to_r) for i, r in enumerate(pieces)]
+    t2_left = [remote(xp.at[x, r], xp.at[x, r], t2s.at[4 + i], t2r.at[4 + i], to_l) for i, r in enumerate(pieces)]
+    t2_on_right = [
+        remote(xp.at[left, pieces[i]], xp.at[left, pieces[i]], t2s.at[8 + i], t2r.at[8 + i], to_r) for i in (0, 1)
+    ]
+    t2_on_left = [
+        remote(xp.at[right, pieces[i]], xp.at[right, pieces[i]], t2s.at[8 + i], t2r.at[8 + i], to_l) for i in (2, 3)
+    ]
 
     def t2_came(group, i, slot):
-        ref = xp.at[group, halves[i]]
+        ref = xp.at[group, pieces[i]]
         remote(ref, ref, t2s.at[slot], t2r.at[slot], to_r).wait_recv()
 
+    for copy in rest_x:
+        copy.wait()
+    for i in range(NX):
+        normed(xloc, row, i)
     row_came(1)
     w_ring.begin(0)
-    row_came(2)
-    row_came(3)
-    w_ring.begin(1)
-    for i in range(2):
+    for i in range(1, 4):
+        row_came(2 * i)
+        row_came(2 * i + 1)
+        w_ring.begin(i)
+    w_ring.step(1, 0)
+    w_ring.step(1, 1)
+    for i in range(4):
         across[i].wait_recv()
         t2_right[i].start()
         t2_left[i].start()
-        row_came(4 + 2 * i)
-        row_came(5 + 2 * i)
-        w_ring.begin(2 + i)
-    for copy in rest_x:
-        copy.wait()
-    for i in range(NX):
-        w_ring.step(1, i)
-        normed(xloc, row, i)
-    t2_came(left, 0, 0)
-    t2_on_right.start()
-    t2_came(right, 1, 3)
-    t2_on_left.start()
+        if i < 2:
+            w_ring.step(1, 2 + i)
+        elif i == 2:
+            w_ring.step(2, 0)
+    w_ring.step(2, 1)
+    for i in range(2):
+        t2_came(left, i, i)
+        t2_on_right[i].start()
+        t2_came(right, 2 + i, 6 + i)
+        t2_on_left[i].start()
+        w_ring.step(2, 2 + i)
     for i in (1, 2, 3):
         wo_right[i].start()
     for i in (3, 0, 1):
         wo_left[i].start()
-    normed(xp, 1 - row, x)
-    t2_came(left, 1, 1)
-    t2_came(right, 0, 2)
     for i in range(4):
-        w_ring.step(2, i)
-        if i == 1:
+        w_ring.step(3, i)
+        if i == 0:
+            normed(xp, 1 - row, x)
+        elif i == 1:
+            t2_came(left, 2, 2)
+            t2_came(left, 3, 3)
             normed(xp, 1 - row, left)
-        elif i == 3:
+        elif i == 2:
+            t2_came(right, 0, 4)
+            t2_came(right, 1, 5)
             normed(xp, 1 - row, right)
     for i in range(4):
-        w_ring.step(3, i)
-    t2_came(far, 0, 4)
-    t2_came(far, 1, 5)
+        t2_came(far, i, 8 + i)
     normed(xp, 1 - row, far)
     wo_came(3, 0, 0)
     wo_on_right[0].start()
@@ -358,18 +369,21 @@
         lambda yo, stream, i: kvbuf.at[yo, i // 2, stream, pl.ds((i % 2) * half_rows, half_rows)],
         sems[6:12],
     )
-    st_ring = Ring(y, c, 2, lambda yo, stream, i: stbuf.at[yo, stream, i], sems[12:18])
+    st_ring = Ring(
+        y, c, 2, lambda yo, stream, i: stbuf.at[yo, stream, pl.ds(i * ST_ROWS // 2, ST_ROWS // 2)], sems[12:18]
+    )
     for kind in range(2):
         one, two = projected(2, kind)
         kvbuf[y, kind, c, :, pl.ds(0, HEAD)] = turned(two, kind).astype(BF16)
         query = turned(one, kind)
         q2[kind, pl.ds(0, TOK)] = jnp.where(lane < PAIR, query, 0.0).astype(BF16)
         q2[kind, pl.ds(TOK, TOK)] = jnp.where(lane >= PAIR, query, 0.0).astype(BF16)
+        if kind == 1:
+            kv_ring.begin(0)
+            kv_ring.begin(1)
         one, two = projected(1, kind)
         kvbuf[y, kind, c, :, pl.ds(HEAD, HEAD)] = two.astype(BF16)
         rec[2, kind] = one.astype(BF16)
-    kv_ring.begin(0)
-    kv_ring.begin(1)
     for kind in range(2):
         one, two = projected(0, kind)
         rec[0, kind] = one.astype(BF16)
@@ -411,7 +425,10 @@
             fresh = jnp.dot(value.astype(F32).T.astype(BF16), k_end, preferred_element_type=F32)
             state = state * jnp.exp(end) + fresh
             total = total + end
-        stbuf[y, c, kind, pl.ds(0, HEAD)] = state.astype(BF16)
+        pack(pair, (c, kind), state, total)
+
+    def pack(buffer, where, state, total):
+        buffer[(*where, pl.ds(0, HEAD))] = state.astype(BF16)
         high = total.astype(BF16)
         rest = total - high.astype(F32)
         middle = rest.astype(BF16)
@@ -420,14 +437,31 @@
         stack = jnp.where(
             index == 0, high.astype(F32), jnp.where(index == 1, middle.astype(F32), low.astype(F32))
         )
-        stbuf[y, c, kind, pl.ds(HEAD, ST_ROWS - HEAD)] = stack.astype(BF16)
+        buffer[(*where, pl.ds(HEAD, ST_ROWS - HEAD))] = stack.astype(BF16)
+
+    def unpack(buffer, where):
+        tail = buffer[(*where, pl.ds(HEAD, ST_ROWS - HEAD))].astype(F32)
+        return buffer[(*where, pl.ds(0, HEAD))].astype(F32), tail[0:1] + tail[1:2] + tail[2:3]
+
+    def pair_came(kind):
+        ref = pair.at[1 - c, kind]
+        remote(ref, ref, prs.at[kind], prr.at[kind], core).wait_recv()
+
+    pair_sends = [
+        remote(pair.at[c, kind], pair.at[c, kind], prs.at[kind], prr.at[kind], core) for kind in range(2)
+    ]
 
     segment(0)
+    pair_sends[0].start()
+    segment(1)
+    pair_sends[1].start()
     kv_ring.step(1, 0)
     kv_ring.step(1, 1)
-    segment(1)
-    kv_ring.step(1, 2)
-    kv_ring.step(1, 3)
+    pair_came(0)
+    pair_came(1)
+    early, early_total = unpack(pair, (0, c))
+    late, late_total = unpack(pair, (1, c))
+    pack(stbuf, (y, c), early * jnp.exp(late_total) + late, early_total + late_total)
     st_ring.begin(0)
     st_ring.begin(1)
 
@@ -437,38 +471,50 @@
 
     kv_ring.wait_other(0)
 
+    ones = jnp.ones((2 * TOK, HEAD), BF16)
+
     def own(kind, carry):
         keys, values = keys_values(y, kind)
-        for part in range(2):
-            rows = pl.ds(part * TOK, TOK)
-            scores = lax.dot_general(q2[kind, rows], keys, NT, preferred_element_type=F32)
-            seen = lax.broadcasted_iota(jnp.int32, (TOK, 2 * TOK), 1) <= (
-                lax.broadcasted_iota(jnp.int32, (TOK, 2 * TOK), 0) + c * TOK
-            )
+        values = jnp.concatenate([values, ones], axis=1)
+        halves_of = [pl.ds(part * TOK, TOK) for part in range(2)]
+        queries = [q2[kind, rows] for rows in halves_of]
+        seen = lax.broadcasted_iota(jnp.int32, (TOK, 2 * TOK), 1) <= (
+            lax.broadcasted_iota(jnp.int32, (TOK, 2 * TOK), 0) + c * TOK
+        )
+        done = []
+        for query in queries:
+            scores = lax.dot_general(query, keys, NT, preferred_element_type=F32)
             scores = jnp.where(seen, scores, -jnp.inf)
-            best = jnp.max(scores, axis=-1, keepdims=True)
-            expo = jnp.exp2((scores - best) * SCORE_LOG2)
-            m_s[kind, rows] = jnp.broadcast_to(best, (TOK, HEAD))
-            l_s[kind, rows] = jnp.broadcast_to(jnp.sum(expo, axis=-1, keepdims=True), (TOK, HEAD))
-            acc[kind, rows] = jnp.dot(expo.astype(BF16), values, preferred_element_type=F32)
+            best = jnp.broadcast_to(jnp.max(scores, axis=-1, keepdims=True), (TOK, HEAD))
+            expo = jnp.exp2((scores - jnp.concatenate([best] * 4, axis=1)) * SCORE_LOG2).astype(BF16)
+            done.append((best, jnp.dot(expo, values, preferred_element_type=F32)))
+        for rows, (best, total) in zip(halves_of, done):
+            m_s[kind, rows] = best
+            acc[kind, rows] = total
         return carry
 
     lax.fori_loop(0, 2, own, 0)
+    kv_ring.step(1, 2)
+    kv_ring.step(1, 3)
 
     def absorb(yo, q_kind, kv_kind):
         keys, values = keys_values(yo, kv_kind)
-        for part in range(2):
-            rows = pl.ds(part * TOK, TOK)
-            scores = lax.dot_general(q2[q_kind, rows], keys, NT, preferred_element_type=F32)
-            old = m_s[q_kind, rows]
+        values = jnp.concatenate([values, ones], axis=1)
+        halves_of = [pl.ds(part * TOK, TOK) for part in range(2)]
+        queries = [q2[q_kind, rows] for rows in halves_of]
+        olds = [m_s[q_kind, rows] for rows in halves_of]
+        sums = [acc[q_kind, rows] for rows in halves_of]
+        done = []
+        for query, old, total in zip(queries, olds, sums):
+            scores = lax.dot_general(query, keys, NT, preferred_element_type=F32)
             best = jnp.maximum(old, jnp.max(scores, axis=-1, keepdims=True))
             scale = jnp.exp2((old - best) * SCORE_LOG2)
-            expo = jnp.exp2((scores - best[:, :1]) * SCORE_LOG2)
+            expo = jnp.exp2((scores - jnp.concatenate([best] * 4, axis=1)) * SCORE_LOG2).astype(BF16)
+            fresh = jnp.dot(expo, values, preferred_element_type=F32)
+            done.append((best, total * jnp.concatenate([scale] * 2, axis=1) + fresh))
+        for rows, (best, total) in zip(halves_of, done):
             m_s[q_kind, rows] = best
-            l_s[q_kind, rows] = l_s[q_kind, rows] * scale + jnp.sum(expo, axis=-1, keepdims=True)
-            acc[q_kind, rows] = acc[q_kind, rows] * scale + jnp.dot(
-                expo.astype(BF16), values, preferred_element_type=F32
-            )
+            acc[q_kind, rows] = total
 
     def process(offset):
         if offset:
@@ -495,123 +541,146 @@
         process(1 - k)
         kv_ring.step(k, 2)
         kv_ring.step(k, 3)
+        process(k - 1)
         st_ring.step(k - 1, 0)
         st_ring.step(k - 1, 1)
-        if k == 3:
+        if k == 2:
             wo_came(3, 1, 1)
             wo_on_right[1].start()
             wo_came(1, 3, 7)
             wo_on_left[1].start()
-        process(k - 1)
+        elif k == 3:
+            wo_came(3, 2, 2)
+            wo_came(1, 0, 4)
+        else:
+            wo_came(3, 3, 3)
+            wo_came(1, 1, 5)
+            wo_came(2, 0, 8)
+            wo_came(2, 2, 10)
+    process(HALF)
     st_ring.step(HALF, 0)
     st_ring.step(HALF, 1)
-    process(HALF)
     for offset in range(NY):
         st_ring.wait_other(offset)
 
-    me = 2 * y + c
-
-    def pass_on(kind, s, state):
-        yo, stream = s // 2, s % 2
-        tail = stbuf[yo, stream, kind, pl.ds(HEAD, ST_ROWS - HEAD)].astype(F32)
-        total = tail[0:1] + tail[1:2] + tail[2:3]
-        return state * jnp.exp(total) + stbuf[yo, stream, kind, pl.ds(0, HEAD)].astype(F32)
+    def pass_on(kind, yo, state):
+        fresh, total = unpack(stbuf, (yo, kind))
+        return state * jnp.exp(total) + fresh
+
+    def within(kind, state):
+        fresh, total = unpack(pair, (0, kind))
+        after = state * jnp.exp(total) + fresh
+        return jnp.where(c == 0, state, after)
 
     nothing = jnp.zeros((HEAD, HEAD), F32)
-    into_low = lax.fori_loop(0, me, functools.partial(pass_on, 0), nothing)
-    all_low = lax.fori_loop(me, 2 * NY, functools.partial(pass_on, 0), into_low)
+    into_low = lax.fori_loop(0, y, functools.partial(pass_on, 0), nothing)
+    all_low = lax.fori_loop(y, NY, functools.partial(pass_on, 0), into_low)
     all_low = all_low * jnp.where(linked, 1.0, 0.0)
-    into_high = lax.fori_loop(0, me, functools.partial(pass_on, 1), all_low)
+    into_high = lax.fori_loop(0, y, functools.partial(pass_on, 1), all_low)
+    into_low, into_high = within(0, into_low), within(1, into_high)
     lam = lam_ref[row]
-
-    def mix_to(same, d):
-        kind = row if same else 1 - row
-        there = (x + d) % NX
-        n = d if same else NX + d
-        where = {"tp": there} if same else {"sp_0": zp, "tp": there}
-        return remote(mixs.at[kind, there], mb.at[x, row], as_.at[n], ar.at[n], where)
-
-    for kind in range(2):
-        state = (into_low if kind == 0 else into_high).astype(BF16)
+    token_halves = (pl.ds(0, TOK // 2), pl.ds(TOK // 2, TOK // 2))
+
+    def mixed(kind):
+        state = jnp.where(kind == 0, into_low, into_high).astype(BF16)
         raw = local[kind] + lax.dot_general(qdec[kind], state, NT, preferred_element_type=F32)
         mean_sq = jnp.mean(raw * raw, axis=-1, keepdims=True)
         rec_mix = (raw * lax.rsqrt(mean_sq + RECUR_EPSILON) * rgain_ref[...]).astype(BF16)
-        raw = acc[kind, pl.ds(0, TOK)] / l_s[kind, pl.ds(0, TOK)] - lam * (
-            acc[kind, pl.ds(TOK, TOK)] / l_s[kind, pl.ds(TOK, TOK)]
-        )
+        low, high = acc[kind, pl.ds(0, TOK)], acc[kind, pl.ds(TOK, TOK)]
+        raw = low[:, :HEAD] / low[:, HEAD:] - lam * (high[:, :HEAD] / high[:, HEAD:])
         mean_sq = jnp.mean(raw * raw, axis=-1, keepdims=True)
         att_mix = (raw * lax.rsqrt(mean_sq + ATTEND_EPSILON) * again_ref[...]).astype(BF16)
-        for i in range(NX):
-            mixs[kind, i, :, pl.ds(0, HEAD)] = rec_mix[i * QUART : (i + 1) * QUART]
-            mixs[kind, i, :, pl.ds(HEAD, HEAD)] = att_mix[i * QUART : (i + 1) * QUART]
-
-    mix_sends = [mix_to(False, d) for d in (2, 1, 3, 0)] + [mix_to(True, d) for d in (2, 1, 3)]
-    for copy in mix_sends:
+        return jnp.concatenate([rec_mix, att_mix], axis=1)
+
+    def hop(group, head, i, slot, where):
+        ref = gm.at[group, head, token_halves[i]]
+        return remote(ref, ref, ms.at[slot], mr.at[slot], where)
+
+    def came(group, head, i, slot):
+        hop(group, head, i, slot, to_r).wait_recv()
+
+    hops = []
+
+    def go(*args):
+        hops.append(hop(*args))
+        hops[-1].start()
+
+    give[...] = mixed(1 - row)
+    gives = [
+        remote(give.at[r], gm.at[x, row, r], ms.at[12 + i], mr.at[12 + i], {"sp_0": zp})
+        for i, r in enumerate(token_halves)
+    ]
+    for copy in gives:
         copy.start()
-    mb[x, row] = mixs[row, x]
-
-    for i in (1, 2, 3):
-        if i != 1:
-            wo_came(3, i, i)
-    for i in (0, 1):
-        wo_came(1, i, 4 + i)
-    for i in range(4):
-        wo_came(2, i, 8 + i)
-    for g in (1, 2, 3):
+    gm[x, row] = mixed(row)
+    go(x, row, 0, 0, to_r)
+    go(x, row, 1, 3, to_l)
+    go(x, row, 1, 1, to_r)
+    go(x, row, 0, 2, to_l)
+    for i in range(2):
+        came(x, 1 - row, i, 12 + i)
+        go(x, 1 - row, i, 6 + i, to_r)
+        go(x, 1 - row, i, 8 + i, to_l)
+
+    def product(group, j):
+        parts = [gm[group, h, :, pl.ds(p * HEAD, HEAD)] for p in range(2) for h in range(2)]
+        weight = wobuf[group, j // 2, :, pl.ds((j % 2) * width, width)]
+        out = jnp.dot(jnp.concatenate(parts, axis=1), weight, preferred_element_type=F32)
+        return out.astype(BF16).astype(F32)
+
+    def wo_ready(offset):
         for i in range(4):
-            ref = wobuf.at[(x + g) % NX, 1 - c, pl.ds(i * HEAD, HEAD)]
-            remote(ref, ref, wops.at[4 * (g - 1) + i], wopr.at[4 * (g - 1) + i], core).wait_recv()
-
-    for d in range(NX):
-        for same in (True, False):
-            if same and d == 0:
-                continue
-            n = d if same else NX + d
-            ref = mb.at[(x + NX - d) % NX, row if same else 1 - row]
-            remote(ref, ref, as_.at[n], ar.at[n], core).wait_recv()
+            ref = wobuf.at[(x + offset) % NX, 1 - c, pl.ds(i * HEAD, HEAD)]
+            n = 4 * (offset - 1) + i
+            remote(ref, ref, wops.at[n], wopr.at[n], core).wait_recv()
 
     width = OUT_HALF // 2
-    groups = [
-        jnp.concatenate([mb[g, h][:, p * HEAD : (p + 1) * HEAD] for p in range(2) for h in range(2)], axis=1)
-        for g in range(NX)
-    ]
-    gathers = []
+    came(left, row, 0, 0)
+    go(left, row, 0, 4, to_r)
+    came(right, row, 1, 3)
+    go(right, row, 1, 5, to_l)
     for j in range(4):
-        total = jnp.zeros((QUART, width), F32)
-        for g in range(NX):
-            weight = wobuf[g, j // 2, :, pl.ds((j % 2) * width, width)]
-            total += jnp.dot(groups[g], weight, preferred_element_type=F32).astype(BF16).astype(F32)
-        cols = pl.ds(j * width, width)
-        out_ref[x, :, cols] = total.astype(BF16)
-        ref = out_ref.at[x, :, cols]
-        gathers.append(remote(ref, ref, gs.at[4 * j], gr.at[4 * j], to_r))
-        gathers.append(remote(ref, ref, gs.at[4 * j + 1], gr.at[4 * j + 1], to_l))
-        gathers[-2].start()
-        gathers[-1].start()
+        sums[:, pl.ds(j * width, width)] = product(x, j)
+    came(left, 1 - row, 0, 6)
+    go(left, 1 - row, 0, 10, to_r)
+    came(right, 1 - row, 1, 9)
+    go(right, 1 - row, 1, 11, to_l)
+    wo_came(2, 1, 9)
+    wo_came(2, 3, 11)
+    for offset in (1, 2, 3):
+        wo_ready(offset)
+    came(left, row, 1, 1)
+    came(right, row, 0, 2)
+    came(left, 1 - row, 1, 7)
+    came(right, 1 - row, 0, 8)
+
+    def near(i, carry):
+        group = jnp.where(i == 0, left, right)
+        for j in range(4):
+            cols = pl.ds(j * width, width)
+            sums[:, cols] = sums[:, cols] + product(group, j)
+        return carry
+
+    lax.fori_loop(0, 2, near, 0)
+    came(far, row, 0, 4)
+    came(far, row, 1, 5)
+    came(far, 1 - row, 0, 10)
+    came(far, 1 - row, 1, 11)
+    puts = []
     for j in range(4):
         cols = pl.ds(j * width, width)
-        ref = out_ref.at[left, :, cols]
-        remote(ref, ref, gs.at[4 * j], gr.at[4 * j], to_r).wait_recv()
-        ref = out_ref.at[left, halves[0], cols]
-        gathers.append(remote(ref, ref, gs.at[4 * j + 2], gr.at[4 * j + 2], to_r))
-        gathers[-1].start()
-        ref = out_ref.at[right, :, cols]
-        remote(ref, ref, gs.at[4 * j + 1], gr.at[4 * j + 1], to_l).wait_recv()
-        ref = out_ref.at[right, halves[1], cols]
-        gathers.append(remote(ref, ref, gs.at[4 * j + 3], gr.at[4 * j + 3], to_l))
-        gathers[-1].start()
-    for j in range(4):
-        cols = pl.ds(j * width, width)
-        for i in range(2):
-            ref = out_ref.at[far, halves[i], cols]
-            remote(ref, ref, gs.at[4 * j + 2 + i], gr.at[4 * j + 2 + i], to_r).wait_recv()
+        out_ref[:, cols] = (sums[:, cols] + product(far, j)).astype(BF16)
+        puts.append(pltpu.make_async_copy(out_ref.at[:, cols], res_ref.at[:, cols], put.at[j]))
+        puts[-1].start()
     w_ring.finish()
     kv_ring.finish()
     st_ring.finish()
-    sent = list(spread.values()) + across + [shifts] + t2_right + t2_left + [t2_on_right, t2_on_left]
-    sent += wo_right + wo_left + wo_on_right + wo_on_left + list(wo_push.values()) + mix_sends + gathers
+    sent = list(spread.values()) + across + [shifts] + t2_right + t2_left + t2_on_right + t2_on_left
+    sent += wo_right + wo_left + wo_on_right + wo_on_left + list(wo_push.values()) + gives + hops + pair_sends
     for copy in sent:
         copy.wait_send()
+    for copy in puts:
+        copy.wait()
 
 
 def per_device(
@@ -624,13 +693,14 @@
     frequency = np.float32(1.0) / np.float32(ROTARY_BASE) ** steps
     frequency = np.concatenate([frequency] * 4)[None].astype(np.float32)
     d_model = tokens_in.shape[1]
-    out = pl.pallas_call(
+    return pl.pallas_call(
         layer_kernel,
         name="layer",
-        out_shape=jax.ShapeDtypeStruct((NX, QUART, d_model), BF16),
+        out_shape=jax.ShapeDtypeStruct((TOK, d_model), BF16),
         in_specs=[HBM] * 15 + [pl.BlockSpec(memory_space=pltpu.SMEM)],
-        out_specs=VM,
+        out_specs=HBM,
         scratch_shapes=[
+            pltpu.VMEM((TOK, d_model), BF16),
             pltpu.VMEM((2, TOK), F32),
             pltpu.VMEM((1, d_model), F32),
             pltpu.VMEM((1, HEAD), F32),
@@ -647,19 +717,21 @@
             pltpu.VMEM((NX, 2, 4 * HEAD, OUT_HALF), BF16),
             pltpu.VMEM((3, 2, TOK, HEAD), BF16),
             pltpu.VMEM((NY, 2, 2, TOK, 2 * HEAD), BF16),
-            pltpu.VMEM((NY, 2, 2, ST_ROWS, HEAD), BF16),
+            pltpu.VMEM((NY, 2, ST_ROWS, HEAD), BF16),
+            pltpu.VMEM((2, 2, ST_ROWS, HEAD), BF16),
             pltpu.VMEM((2, 2 * TOK, HEAD), BF16),
             pltpu.VMEM((2, 2 * TOK, HEAD), F32),
-            pltpu.VMEM((2, 2 * TOK, HEAD), F32),
-            pltpu.VMEM((2, 2 * TOK, HEAD), F32),
+            pltpu.VMEM((2, TOK, HEAD), F32),
+            pltpu.VMEM((2, 2 * TOK, 2 * HEAD), F32),
             pltpu.VMEM((2, TOK, HEAD), F32),
             pltpu.VMEM((2, TOK, HEAD), BF16),
-            pltpu.VMEM((2, NX, QUART, 2 * HEAD), BF16),
-            pltpu.VMEM((NX, 2, QUART, 2 * HEAD), BF16),
+            pltpu.VMEM((TOK, 2 * HEAD), BF16),
+            pltpu.VMEM((NX, 2, TOK, 2 * HEAD), BF16),
+            pltpu.VMEM((TOK, d_model), F32),
             DMA((26,)),
-            DMA((2,)), DMA((2,)), DMA((6,)), DMA((6,)), DMA((1,)), DMA((1,)),
+            DMA((4,)), DMA((4,)), DMA((12,)), DMA((12,)), DMA((1,)), DMA((1,)),
             DMA((NZ - 1,)), DMA((NZ - 1,)), DMA((12,)), DMA((12,)), DMA((12,)), DMA((12,)),
-            DMA((2 * NX,)), DMA((2 * NX,)), DMA((16,)), DMA((16,)),
+            DMA((14,)), DMA((14,)), DMA((4,)), DMA((2,)), DMA((2,)),
             *ring_sems(4), *ring_sems(4), *ring_sems(2),
         ],
         compiler_params=pltpu.CompilerParams(
@@ -671,7 +743,6 @@
         decay_shift, norm_gain[None], jnp.asarray(frequency), floor_gap.reshape(2, HEAD),
         rec_gain[None], att_gain[None], lambda_head,
     )
-    return out.reshape(TOK, d_model)
 
 
 def solution(mesh):

time: 103 us -> 95.3 us (0.925)
  Pallas kernels: 99.7 us -> 92.8 us
    pallas_call x1, Pallas kernels: 99.7 us -> 92.8 us  [per_device(): pl.pallas_call(layer_kernel, name='layer', out_shape=jax.ShapeDtypeStruct...]
where the time goes in v3:
time: 95.3 us; the launch traced here: 95.1 us
  Pallas kernels  92.8 us (97%)
  local copies, waits for them, and re-layouts  2.3 us (2%)
    pallas_call x1, Pallas kernels, per_device(): pl.pallas_call(layer_kernel, name='layer', out_shape=jax.ShapeDtypeStruct...  92.8 us
    unnamed x1, local copies, waits for them, and re-layouts  2.3 us

profile of v3, /device:TPU:1, one launch (start us, length us, event | category | flops | bytes accessed | tf_op | source)
XLA Modules:
  0.0 95.1 jit_solution(16518814607164119268)
XLA Ops:
  0.0 92.8 %layer.1 = bf16[256,2048]{1,0:T(8,128)(2,1)} custom-call(bf16[4,64,2048]{2,1,0:T(8,128)(2,1)} %bitcast.5, bf16[16,256]{1,0:T(8,128)(2,1)} %wq_ref.1, bf16[16,256]{1,0:T(8,128)(2,1)} %wf_ref.1, bf16[16,256]{1,0:T(8,128)(2,1)} %wi_ref.1, bf16[16,256]{1,0:T(8,128)(2,1)} %wv_ref.1, bf16[16,256]{1,0:T(8,128)(2,1)} %waq_ref.1, bf16[16,256]{1,0:T(8,128)(2,1)} %wak_ref.1, ...), custom_call_target="tpu_custom_call" | custom-call | tf_op jit(solution)/shard_map/layer/pallas_call | solution.py:696
  92.8 2.3 %copy.18 = bf16[256,2048]{1,0:T(8,128)(2,1)} copy(bf16[256,2048]{1,0:T(8,128)(2,1)} %layer.1) | data formatting | bytes 2097152

commit v4 on v3

--- a/solution.py
+++ b/solution.py
@@ -285,51 +285,15 @@
         normed(xloc, row, i)
     row_came(1)
     w_ring.begin(0)
-    for i in range(1, 4):
+    for i in range(1, 3):
         row_came(2 * i)
         row_came(2 * i + 1)
         w_ring.begin(i)
     w_ring.step(1, 0)
+    row_came(6)
+    row_came(7)
+    w_ring.begin(3)
     w_ring.step(1, 1)
-    for i in range(4):
-        across[i].wait_recv()
-        t2_right[i].start()
-        t2_left[i].start()
-        if i < 2:
-            w_ring.step(1, 2 + i)
-        elif i == 2:
-            w_ring.step(2, 0)
-    w_ring.step(2, 1)
-    for i in range(2):
-        t2_came(left, i, i)
-        t2_on_right[i].start()
-        t2_came(right, 2 + i, 6 + i)
-        t2_on_left[i].start()
-        w_ring.step(2, 2 + i)
-    for i in (1, 2, 3):
-        wo_right[i].start()
-    for i in (3, 0, 1):
-        wo_left[i].start()
-    for i in range(4):
-        w_ring.step(3, i)
-        if i == 0:
-            normed(xp, 1 - row, x)
-        elif i == 1:
-            t2_came(left, 2, 2)
-            t2_came(left, 3, 3)
-            normed(xp, 1 - row, left)
-        elif i == 2:
-            t2_came(right, 0, 4)
-            t2_came(right, 1, 5)
-            normed(xp, 1 - row, right)
-    for i in range(4):
-        t2_came(far, i, 8 + i)
-    normed(xp, 1 - row, far)
-    wo_came(3, 0, 0)
-    wo_on_right[0].start()
-    wo_came(1, 2, 6)
-    wo_on_left[0].start()
-
     lane = lax.broadcasted_iota(jnp.int32, (TOK, HEAD), 1)
     first = (lane % PAIR) < (PAIR // 2)
     place = (2 * y + c) * TOK + lax.broadcasted_iota(jnp.int32, (TOK, HEAD), 0)
@@ -348,11 +312,62 @@
         )
         return values * m_s[kind, pl.ds(0, TOK)] + swapped * l_s[kind, pl.ds(0, TOK)]
 
+    def tokens_came(i):
+        across[i].wait_recv()
+        t2_right[i].start()
+        t2_left[i].start()
+
+    def from_left(i):
+        t2_came(left, i, i)
+        t2_on_right[i].start()
+
+    def from_right(i):
+        t2_came(right, i, 4 + i)
+        t2_on_left[i - 2].start()
+
+    w_ring.step(1, 2)
+    tokens_came(0)
+    w_ring.step(1, 3)
+    tokens_came(1)
+    w_ring.step(2, 0)
+    tokens_came(2)
+    w_ring.step(2, 1)
+    tokens_came(3)
+    w_ring.step(2, 2)
+    normed(xp, 1 - row, x)
+    from_left(0)
+    w_ring.step(2, 3)
+    from_left(1)
+    from_right(2)
+    w_ring.step(3, 0)
+    from_right(3)
+    for i in (1, 2, 3):
+        wo_right[i].start()
+    for i in (3, 0, 1):
+        wo_left[i].start()
+    w_ring.step(3, 1)
+    t2_came(left, 2, 2)
+    t2_came(left, 3, 3)
+    normed(xp, 1 - row, left)
+    w_ring.step(3, 2)
+    t2_came(right, 0, 4)
+    t2_came(right, 1, 5)
+    normed(xp, 1 - row, right)
+    w_ring.step(3, 3)
+    w_ring.step(4, 0)
+    w_ring.step(4, 2)
+    for i in range(4):
+        t2_came(far, i, 8 + i)
+    normed(xp, 1 - row, far)
+    wo_came(3, 0, 0)
+    wo_on_right[0].start()
+    wo_came(1, 2, 6)
+    wo_on_left[0].start()
     shifts.wait_recv()
     dso[pl.ds(row, 1)] = ds_ref[pl.ds(row, 1)]
     dso[pl.ds(1 - row, 1)] = dsp[pl.ds(row, 1)]
-    for i in range(4):
-        w_ring.step(4, i)
+    w_ring.step(4, 1)
+    w_ring.step(4, 3)
     for offset in range(NY):
         w_ring.wait_other(offset)
 
@@ -378,12 +393,12 @@
         query = turned(one, kind)
         q2[kind, pl.ds(0, TOK)] = jnp.where(lane < PAIR, query, 0.0).astype(BF16)
         q2[kind, pl.ds(TOK, TOK)] = jnp.where(lane >= PAIR, query, 0.0).astype(BF16)
-        if kind == 1:
-            kv_ring.begin(0)
-            kv_ring.begin(1)
         one, two = projected(1, kind)
         kvbuf[y, kind, c, :, pl.ds(HEAD, HEAD)] = two.astype(BF16)
         rec[2, kind] = one.astype(BF16)
+        if kind == 0:
+            kv_ring.begin(0)
+            kv_ring.begin(1)
     for kind in range(2):
         one, two = projected(0, kind)
         rec[0, kind] = one.astype(BF16)
@@ -457,14 +472,6 @@
     pair_sends[1].start()
     kv_ring.step(1, 0)
     kv_ring.step(1, 1)
-    pair_came(0)
-    pair_came(1)
-    early, early_total = unpack(pair, (0, c))
-    late, late_total = unpack(pair, (1, c))
-    pack(stbuf, (y, c), early * jnp.exp(late_total) + late, early_total + late_total)
-    st_ring.begin(0)
-    st_ring.begin(1)
-
     def keys_values(yo, kind):
         both = kvbuf[yo, kind].reshape(2 * TOK, 2 * HEAD)
         return both[:, :HEAD], both[:, HEAD:]
@@ -496,6 +503,13 @@
     lax.fori_loop(0, 2, own, 0)
     kv_ring.step(1, 2)
     kv_ring.step(1, 3)
+    pair_came(0)
+    pair_came(1)
+    early, early_total = unpack(pair, (0, c))
+    late, late_total = unpack(pair, (1, c))
+    pack(stbuf, (y, c), early * jnp.exp(late_total) + late, early_total + late_total)
+    st_ring.begin(0)
+    st_ring.begin(1)
 
     def absorb(yo, q_kind, kv_kind):
         keys, values = keys_values(yo, kv_kind)

time: 95.3 us -> 93.7 us (0.983)
  Pallas kernels: 92.8 us -> 91.2 us
    pallas_call x1, Pallas kernels: 92.8 us -> 91.2 us  [per_device(): pl.pallas_call(layer_kernel, name='layer', out_shape=jax.ShapeDtypeStruct...]
where the time goes in v4:
time: 93.7 us; the launch traced here: 93.5 us
  Pallas kernels  91.2 us (97%)
  local copies, waits for them, and re-layouts  2.3 us (2%)
    pallas_call x1, Pallas kernels, per_device(): pl.pallas_call(layer_kernel, name='layer', out_shape=jax.ShapeDtypeStruct...  91.2 us
    unnamed x1, local copies, waits for them, and re-layouts  2.3 us

profile of v4, /device:TPU:1, one launch (start us, length us, event | category | flops | bytes accessed | tf_op | source)
XLA Modules:
  0.0 93.5 jit_solution(2918878957724495087)
XLA Ops:
  0.0 91.2 %layer.1 = bf16[256,2048]{1,0:T(8,128)(2,1)} custom-call(bf16[4,64,2048]{2,1,0:T(8,128)(2,1)} %bitcast.5, bf16[16,256]{1,0:T(8,128)(2,1)} %wq_ref.1, bf16[16,256]{1,0:T(8,128)(2,1)} %wf_ref.1, bf16[16,256]{1,0:T(8,128)(2,1)} %wi_ref.1, bf16[16,256]{1,0:T(8,128)(2,1)} %wv_ref.1, bf16[16,256]{1,0:T(8,128)(2,1)} %waq_ref.1, bf16[16,256]{1,0:T(8,128)(2,1)} %wak_ref.1, ...), custom_call_target="tpu_custom_call" | custom-call | tf_op jit(solution)/shard_map/layer/pallas_call | solution.py:710
  91.2 2.3 %copy.18 = bf16[256,2048]{1,0:T(8,128)(2,1)} copy(bf16[256,2048]{1,0:T(8,128)(2,1)} %layer.1) | data formatting | bytes 2097152

commit v5 on v4

--- a/solution.py
+++ b/solution.py
@@ -593,7 +593,7 @@
     into_high = lax.fori_loop(0, y, functools.partial(pass_on, 1), all_low)
     into_low, into_high = within(0, into_low), within(1, into_high)
     lam = lam_ref[row]
-    token_halves = (pl.ds(0, TOK // 2), pl.ds(TOK // 2, TOK // 2))
+    token_parts = tuple(pl.ds(i * (TOK // 4), TOK // 4) for i in range(4))
 
     def mixed(kind):
         state = jnp.where(kind == 0, into_low, into_high).astype(BF16)
@@ -607,7 +607,7 @@
         return jnp.concatenate([rec_mix, att_mix], axis=1)
 
     def hop(group, head, i, slot, where):
-        ref = gm.at[group, head, token_halves[i]]
+        ref = gm.at[group, head, token_parts[i]]
         return remote(ref, ref, ms.at[slot], mr.at[slot], where)
 
     def came(group, head, i, slot):
@@ -621,20 +621,32 @@
 
     give[...] = mixed(1 - row)
     gives = [
-        remote(give.at[r], gm.at[x, row, r], ms.at[12 + i], mr.at[12 + i], {"sp_0": zp})
-        for i, r in enumerate(token_halves)
-    ]
-    for copy in gives:
-        copy.start()
+        remote(give.at[r], gm.at[x, row, r], ms.at[24 + i], mr.at[24 + i], {"sp_0": zp})
+        for i, r in enumerate(token_parts)
+    ]
+    for i in (0, 2, 1, 3):
+        gives[i].start()
     gm[x, row] = mixed(row)
-    go(x, row, 0, 0, to_r)
-    go(x, row, 1, 3, to_l)
-    go(x, row, 1, 1, to_r)
-    go(x, row, 0, 2, to_l)
-    for i in range(2):
-        came(x, 1 - row, i, 12 + i)
-        go(x, 1 - row, i, 6 + i, to_r)
-        go(x, 1 - row, i, 8 + i, to_l)
+    for i in range(4):
+        go(x, row, i, i, to_r)
+        go(x, row, (i + 2) % 4, 4 + (i + 2) % 4, to_l)
+
+    def given(i):
+        came(x, 1 - row, i, 24 + i)
+        go(x, 1 - row, i, 12 + i, to_r)
+        go(x, 1 - row, i, 16 + i, to_l)
+
+    def relay(head, base, i):
+        came(left, head, i, base + i)
+        go(left, head, i, base + 8 + i, to_r)
+        came(right, head, 2 + i, base + 6 + i)
+        go(right, head, 2 + i, base + 10 + i, to_l)
+
+    relay(row, 0, 0)
+    given(0)
+    relay(row, 0, 1)
+    for i in (2, 1, 3):
+        given(i)
 
     def product(group, j):
         parts = [gm[group, h, :, pl.ds(p * HEAD, HEAD)] for p in range(2) for h in range(2)]
@@ -649,24 +661,18 @@
             remote(ref, ref, wops.at[n], wopr.at[n], core).wait_recv()
 
     width = OUT_HALF // 2
-    came(left, row, 0, 0)
-    go(left, row, 0, 4, to_r)
-    came(right, row, 1, 3)
-    go(right, row, 1, 5, to_l)
     for j in range(4):
         sums[:, pl.ds(j * width, width)] = product(x, j)
-    came(left, 1 - row, 0, 6)
-    go(left, 1 - row, 0, 10, to_r)
-    came(right, 1 - row, 1, 9)
-    go(right, 1 - row, 1, 11, to_l)
+    relay(1 - row, 12, 0)
+    relay(1 - row, 12, 1)
     wo_came(2, 1, 9)
     wo_came(2, 3, 11)
     for offset in (1, 2, 3):
         wo_ready(offset)
-    came(left, row, 1, 1)
-    came(right, row, 0, 2)
-    came(left, 1 - row, 1, 7)
-    came(right, 1 - row, 0, 8)
+    for i in range(2):
+        for base, head in ((0, row), (12, 1 - row)):
+            came(left, head, 2 + i, base + 2 + i)
+            came(right, head, i, base + 4 + i)
 
     def near(i, carry):
         group = jnp.where(i == 0, left, right)
@@ -676,10 +682,9 @@
         return carry
 
     lax.fori_loop(0, 2, near, 0)
-    came(far, row, 0, 4)
-    came(far, row, 1, 5)
-    came(far, 1 - row, 0, 10)
-    came(far, 1 - row, 1, 11)
+    for i in range(4):
+        came(far, row, i, 8 + i)
+        came(far, 1 - row, i, 20 + i)
     puts = []
     for j in range(4):
         cols = pl.ds(j * width, width)
@@ -745,7 +750,7 @@
             DMA((26,)),
             DMA((4,)), DMA((4,)), DMA((12,)), DMA((12,)), DMA((1,)), DMA((1,)),
             DMA((NZ - 1,)), DMA((NZ - 1,)), DMA((12,)), DMA((12,)), DMA((12,)), DMA((12,)),
-            DMA((14,)), DMA((14,)), DMA((4,)), DMA((2,)), DMA((2,)),
+            DMA((28,)), DMA((28,)), DMA((4,)), DMA((2,)), DMA((2,)),
             *ring_sems(4), *ring_sems(4), *ring_sems(2),
         ],
         compiler_params=pltpu.CompilerParams(

time: 93.7 us -> 93.9 us (level)
  no operation moved by 1% of the time
where the time goes in v5:
time: 93.9 us; the launch traced here: 93.7 us
  Pallas kernels  91.4 us (97%)
  local copies, waits for them, and re-layouts  2.3 us (2%)
    pallas_call x1, Pallas kernels, per_device(): pl.pallas_call(layer_kernel, name='layer', out_shape=jax.ShapeDtypeStruct...  91.4 us
    unnamed x1, local copies, waits for them, and re-layouts  2.3 us

profile of v5, /device:TPU:1, one launch (start us, length us, event | category | flops | bytes accessed | tf_op | source)
XLA Modules:
  0.0 93.7 jit_solution(6822367807662019399)
XLA Ops:
  0.0 91.4 %layer.1 = bf16[256,2048]{1,0:T(8,128)(2,1)} custom-call(bf16[4,64,2048]{2,1,0:T(8,128)(2,1)} %bitcast.5, bf16[16,256]{1,0:T(8,128)(2,1)} %wq_ref.1, bf16[16,256]{1,0:T(8,128)(2,1)} %wf_ref.1, bf16[16,256]{1,0:T(8,128)(2,1)} %wi_ref.1, bf16[16,256]{1,0:T(8,128)(2,1)} %wv_ref.1, bf16[16,256]{1,0:T(8,128)(2,1)} %waq_ref.1, bf16[16,256]{1,0:T(8,128)(2,1)} %wak_ref.1, ...), custom_call_target="tpu_custom_call" | custom-call | tf_op jit(solution)/shard_map/layer/pallas_call | solution.py:715
  91.4 2.3 %copy.18 = bf16[256,2048]{1,0:T(8,128)(2,1)} copy(bf16[256,2048]{1,0:T(8,128)(2,1)} %layer.1) | data formatting | bytes 2097152
